TPU v7x, 32 devices: a whole 2x2x4 slice. The times are simulated.
32 devices in a mesh: rep: 2 (over x), fs: 8 (over z, y), tp: 2 (over core).
Axes of the slice: x: 2, y: 2, z: 4, core: 2. Of those that a mesh axis runs over, the one named last changes fastest.
Arguments:
- inputs: bfloat16 [2048, 2048], P(('rep', 'fs'), 'tp'), may hold values from -6 to 6
- cotangent: bfloat16 [2048, 2048], P(('rep', 'fs'), 'tp'), may hold values from -8 to 8
- gate_weight: bfloat16 [2048, 2816], P('fs', 'tp'), may hold values from -0.125 to 0.125
- up_weight: bfloat16 [2048, 2816], P('fs', 'tp'), may hold values from -0.125 to 0.125
- down_weight: bfloat16 [2816, 2048], P('tp', 'fs'), may hold values from -0.109375 to 0.109375
Outputs:
- grad_inputs: bfloat16 [2048, 2048], P(('rep', 'fs'), 'tp')
- grad_gate_weight: float32 [2048, 2816], P('fs', 'tp')
- grad_up_weight: float32 [2048, 2816], P('fs', 'tp')
- grad_down_weight: float32 [2816, 2048], P('tp', 'fs')
All inputs are finite; a program needn't handle non-finite values.
Results may differ from a plain program's by a relative error of at most 0.014.
Values may be sent and summed in bfloat16 or wider, within the bound.
A program may use at most 64 MiB of HBM per device.

v0:
```python
import functools

import jax
import jax.numpy as jnp
from jax import lax
from jax.experimental import pallas as pl
from jax.experimental.pallas import tpu as pltpu
from jax.sharding import PartitionSpec as P

MESH = pl.DeviceIdType.MESH


def enter(n_rep, n_fs, n_tp):
    barrier = pltpu.get_barrier_semaphore()
    for axis, n in (("rep", n_rep), ("fs", n_fs), ("tp", n_tp)):
        me = lax.axis_index(axis)
        for k in range(1, n):
            pl.semaphore_signal(
                barrier, inc=1, device_id={axis: lax.rem(me + k, n)}, device_id_type=MESH
            )
    pl.semaphore_wait(barrier, n_rep + n_fs + n_tp - 3)


class Sender:
    def __init__(self, sems):
        self.sems, self.used, self.pending = sems, 0, []

    def run(self, build, when):
        if when is None:
            build().start()
        else:
            pl.when(when)(lambda: build().start())

    def send(self, src, dst, recv_sem, axis, peer, when=None):
        def build(at=self.used):
            return pltpu.make_async_remote_copy(
                src_ref=src,
                dst_ref=dst,
                send_sem=self.sems.at[at],
                recv_sem=recv_sem,
                device_id={axis: peer},
                device_id_type=MESH,
            )

        self.used += 1
        self.run(build, when)
        self.pending.append((lambda: build().wait_send(), when))

    def local(self, src, dst):
        def build(at=self.used):
            return pltpu.make_async_copy(src, dst, self.sems.at[at])

        self.used += 1
        self.run(build, None)
        self.pending.append((lambda: build().wait(), None))

    def finish(self):
        for wait, when in self.pending:
            if when is None:
                wait()
            else:
                pl.when(when)(wait)


def arrived(slot, recv_sem, when=None):
    def wait():
        pltpu.make_async_copy(slot, slot, recv_sem).wait()

    if when is None:
        wait()
    else:
        pl.when(when)(wait)


def near_first(n):
    return sorted(range(1, n), key=lambda k: min(k, n - k))


def split_weights(weights, w_ref):
    n_fs, n_rep, half, depth = w_ref.shape
    units = weights[2].shape[0] // n_fs
    turned = [weights[0][...].T, weights[1][...].T, weights[2][...]]
    for owner in range(n_fs):
        for i, value in enumerate(turned):
            for h in range(n_rep):
                low, high = max(i * units, h * half), min((i + 1) * units, (h + 1) * half)
                if low < high:
                    start = owner * units - i * units
                    w_ref[owner, h, low - h * half : high - h * half] = value[
                        start + low : start + high
                    ]
        used = 3 * units - (n_rep - 1) * half
        w_ref[owner, n_rep - 1, used:] = jnp.zeros((half - used, depth), w_ref.dtype)


def gather_kernel(
    sizes, x_ref, c_ref, *refs
):
    *weights, x_out, c_out, w_out, w_ref, sends, act_recv, w_recv = refs
    n_rep, n_fs, n_tp, n_y = sizes
    n_z = n_fs // n_y
    rep, fs, tp = (lax.axis_index(axis) for axis in ("rep", "fs", "tp"))
    z, y = fs // n_y, lax.rem(fs, n_y)
    width = x_ref.shape[1]
    depth = w_ref.shape[3]
    enter(n_rep, n_fs, n_tp)
    out = Sender(sends)
    acts = ((x_ref, x_out), (c_ref, c_out))

    def act_slot(a, owner, part):
        return acts[a][1].at[owner, :, pl.ds(pl.multiple_of(part * width, width), width)]

    def w_slot(half, owner):
        if depth % 128 == 0:
            return w_out.at[half, :, pl.ds(pl.multiple_of(owner * depth, depth), depth)]
        return w_out.at[half, owner]

    def act_send(a, owner, src, axis, peer, when=None):
        out.send(src, act_slot(a, owner, tp), act_recv.at[a, owner, tp], axis, peer, when)

    def to_tp(a, owner, src, when=None):
        for k in range(1, n_tp):
            act_send(a, owner, src, "tp", lax.rem(tp + k, n_tp), when)

    def to_y(a, owner, src, when=None):
        for k in range(1, n_y):
            act_send(a, owner, src, "fs", z * n_y + lax.rem(y + k, n_y), when)

    for a in range(2):
        src = acts[a][0]
        to_y(a, fs, src)
        act_send(a, fs, src, "fs", fs + n_y, z + 1 < n_z)
        act_send(a, fs, src, "fs", fs - n_y, z >= 1)
    for a in range(2):
        to_tp(a, fs, acts[a][0])
        out.local(acts[a][0], act_slot(a, fs, tp))
    if len(weights) == 1:
        w_ref = weights[0]
    else:
        split_weights(weights, w_ref)
    offsets = near_first(n_fs)
    soon, late = offsets[: len(offsets) // 2], offsets[len(offsets) // 2 :]
    if n_z < 3:
        soon, late = [], offsets

    def send_weights(group):
        for k in group:
            peer = lax.rem(fs + k, n_fs)
            out.send(w_ref.at[peer, rep], w_slot(rep, fs), w_recv.at[rep, fs], "fs", peer)

    if n_z < 3:
        send_weights(late)
    for k in range(1, n_rep):
        out.send(
            w_ref.at[fs, rep], w_slot(rep, fs), w_recv.at[rep, fs], "rep", lax.rem(rep + k, n_rep)
        )
    out.local(w_ref.at[fs, rep], w_slot(rep, fs))

    def swap_weights(group):
        for k in group:
            owner = lax.rem(fs + n_fs - k, n_fs)
            slot = w_slot(rep, owner)
            arrived(slot, w_recv.at[rep, owner])
            for j in range(1, n_rep):
                peer = lax.rem(rep + j, n_rep)
                out.send(slot, slot, w_recv.at[rep, owner], "rep", peer)

    for k in range(1, n_z):
        if k == n_z - 1:
            swap_weights(soon)
        for a in range(2):
            for here, onward, step in (
                (z >= k, z + 1 < n_z, -1), (z + k < n_z, z >= 1, 1)
            ):
                owner = fs + step * k * n_y
                slot = act_slot(a, owner, tp)
                arrived(slot, act_recv.at[a, owner, tp], here)
                if k < n_z - 1:
                    act_send(
                        a, owner, slot, "fs", fs - step * n_y, jnp.logical_and(here, onward)
                    )
                to_y(a, owner, slot, here)
                to_tp(a, owner, slot, here)
        if n_z >= 3 and k == 1:
            send_weights(soon)
        if n_z >= 3 and k == n_z - 2:
            send_weights(late)
    swap_weights(late)
    for kz in [0] + near_first(n_z):
        for ky in range(1, n_y):
            owner = lax.rem(z + n_z - kz, n_z) * n_y + lax.rem(y + ky, n_y)
            for a in range(2):
                slot = act_slot(a, owner, tp)
                arrived(slot, act_recv.at[a, owner, tp])
                to_tp(a, owner, slot)
    for j in range(1, n_rep):
        half = lax.rem(rep + j, n_rep)
        for k in range(n_fs):
            owner = lax.rem(fs + k, n_fs)
            arrived(w_slot(half, owner), w_recv.at[half, owner])
    for j in range(1, n_tp):
        part = lax.rem(tp + j, n_tp)
        for k in range(n_fs):
            owner = lax.rem(fs + k, n_fs)
            for a in range(2):
                arrived(act_slot(a, owner, part), act_recv.at[a, owner, part])
    out.finish()


def scatter_kernel(
    sizes, d_ref, w_ref, g_ref, x_ref, g_out,
    p, p_in, q, y_in, r, x_in, g_in, g_sum, sends, p_recv, y_recv, x_recv, g_recv, gx_recv,
):
    n_rep, n_fs, n_tp, n_y = sizes
    n_z = n_fs // n_y
    f32, bf16 = jnp.float32, jnp.bfloat16
    rep, fs, tp = (lax.axis_index(axis) for axis in ("rep", "fs", "tp"))
    z, y = fs // n_y, lax.rem(fs, n_y)
    rows, width = x_ref.shape
    depth = g_sum.shape[2]
    enter(n_rep, n_fs, n_tp)
    out = Sender(sends)
    order = near_first(n_fs) + [0]
    zs = near_first(n_z) + [0]

    def columns(part, size):
        return pl.ds(pl.multiple_of(part * size, size), size)

    def g_part(owner, half):
        if depth % 128 == 0:
            return g_ref.at[half, :, columns(owner, depth)]
        return g_ref.at[half, owner]

    for k in order:
        owner = lax.rem(fs + k, n_fs)
        for j in range(1, n_rep):
            peer = lax.rem(rep + j, n_rep)
            out.send(
                g_part(owner, peer), g_in.at[j - 1, owner], g_recv.at[j - 1, owner], "rep", peer
            )
    blocks = [(kz, ky) for ky in list(range(1, n_y)) + [0] for kz in zs]

    def owner_of(kz, ky):
        return lax.rem(z + kz, n_z) * n_y + lax.rem(y + ky, n_y)

    for block in blocks:
        owner = owner_of(*block)
        p[owner] = jnp.dot(
            d_ref[owner], w_ref[: d_ref.shape[2]], preferred_element_type=f32
        ).astype(bf16)
        for j in range(1, n_tp):
            peer = lax.rem(tp + j, n_tp)
            out.send(
                p.at[owner, :, columns(peer, width)],
                p_in.at[j - 1, owner],
                p_recv.at[j - 1, owner],
                "tp",
                peer,
            )

    def pair_sum(owner):
        total = p[owner, :, columns(tp, width)].astype(f32)
        for j in range(n_tp - 1):
            arrived(p_in.at[j, owner], p_recv.at[j, owner])
            total = total + p_in[j, owner].astype(f32)
        return total

    def g_step(k):
        owner = lax.rem(fs + k, n_fs)
        total = g_part(owner, rep)[...].astype(f32)
        for j in range(n_rep - 1):
            arrived(g_in.at[j, owner], g_recv.at[j, owner])
            total = total + g_in[j, owner].astype(f32)
        g_sum[owner] = total.astype(bf16)
        slot = g_out.at[fs, rep]
        if k:
            out.send(g_sum.at[owner], slot, gx_recv.at[rep, fs], "fs", owner)
        else:
            out.local(g_sum.at[owner], slot)
            for j in range(1, n_rep):
                out.send(
                    g_sum.at[owner], slot, gx_recv.at[rep, fs], "rep", lax.rem(rep + j, n_rep)
                )

    for kz, ky in blocks:
        if ky:
            owner = owner_of(kz, ky)
            q[owner] = pair_sum(owner).astype(bf16)
            at = (ky - 1, lax.rem(z + kz, n_z))
            out.send(
                q.at[owner], y_in.at[at], y_recv.at[at], "fs", z * n_y + lax.rem(y + ky, n_y)
            )
    def x_step(kz):
        owner = owner_of(kz, 0)
        z_to = lax.rem(z + kz, n_z)
        total = pair_sum(owner)
        for ky in range(1, n_y):
            at = (ky - 1, z_to)
            arrived(y_in.at[at], y_recv.at[at])
            total = total + y_in[at].astype(f32)
        if kz:
            r[z_to] = total.astype(bf16)
            out.send(r.at[z_to], x_in.at[z], x_recv.at[z], "fs", owner)
        else:
            x_in[z] = total.astype(bf16)

    def g_forward(k):
        if k:
            owner = lax.rem(fs + n_fs - k, n_fs)
            slot = g_out.at[owner, rep]
            arrived(slot, gx_recv.at[rep, owner])
            for j in range(1, n_rep):
                out.send(slot, slot, gx_recv.at[rep, owner], "rep", lax.rem(rep + j, n_rep))

    for i, kz in enumerate(zs):
        for k in order[i * n_y : (i + 1) * n_y]:
            g_step(k)
        x_step(kz)
        if i:
            for k in order[(i - 1) * n_y : i * n_y]:
                g_forward(k)
    for k in order[-n_y:]:
        g_forward(k)
    for kz in near_first(n_z):
        z_from = lax.rem(z + n_z - kz, n_z)
        arrived(x_in.at[z_from], x_recv.at[z_from])
    total = x_in[0].astype(f32)
    for k in range(1, n_z):
        total = total + x_in[k].astype(f32)
    x_ref[...] = total.astype(bf16)
    for j in range(1, n_rep):
        half = lax.rem(rep + j, n_rep)
        for k in range(n_fs):
            owner = lax.rem(fs + k, n_fs)
            arrived(g_out.at[owner, half], gx_recv.at[half, owner])
    out.finish()


VMEM = pl.BlockSpec(memory_space=pltpu.VMEM)
ANY = pl.BlockSpec(memory_space=pl.ANY)
DMA = pltpu.SemaphoreType.DMA


def per_device(n_rep, n_fs, n_tp, x, c, gate_weight, up_weight, down_weight):
    bf16, f32 = jnp.bfloat16, jnp.float32
    n_y = max(k for k in range(1, n_fs + 1) if n_fs % k == 0 and k * k <= n_fs)
    n_z = n_fs // n_y
    tokens, width = x.shape
    depth, hidden_tp = gate_weight.shape
    model = width * n_tp
    units = hidden_tp // n_fs
    step = 16 * n_rep
    rows = -(-3 * units // step) * step
    half = rows // n_rep

    weights = [gate_weight, up_weight, down_weight]
    if units % 16 or depth % 128 or 3 * units <= rows - half:
        blocks = [gate_weight.T, up_weight.T, down_weight]
        blocks = [v.reshape(n_fs, units, depth) for v in blocks]
        blocks.append(jnp.zeros((n_fs, rows - 3 * units, depth), bf16))
        weights = [jnp.concatenate(blocks, axis=1).reshape(n_fs, n_rep, half, depth)]
    aligned = depth % 128 == 0
    w_shape = (n_rep, half, model) if aligned else (n_rep, n_fs, half, depth)
    n_sends = (
        2 * (2 + (2 * n_z - 1) * (n_y - 1) + (2 * n_z - 1) * (n_tp - 1) + 2 * n_z + n_fs * (n_tp - 1) + 1)
        + (n_fs - 1) + n_fs * (n_rep - 1) + 1
    )
    x_all, c_all, w_all = pl.pallas_call(
        functools.partial(gather_kernel, (n_rep, n_fs, n_tp, n_y)),
        out_shape=(
            jax.ShapeDtypeStruct((n_fs, tokens, model), bf16),
            jax.ShapeDtypeStruct((n_fs, tokens, model), bf16),
            jax.ShapeDtypeStruct(w_shape, bf16),
        ),
        in_specs=[VMEM] * (2 + len(weights)),
        out_specs=(ANY,) * 3,
        scratch_shapes=[pltpu.VMEM((n_fs, n_rep, half, depth), bf16), DMA((n_sends,)), DMA((2, n_fs, n_tp)), DMA((n_rep, n_fs))],
        compiler_params=pltpu.CompilerParams(collective_id=0, has_side_effects=True),
    )(x, c, *weights)
    x_all, c_all = (v.reshape(n_fs * tokens, model) for v in (x_all, c_all))
    if not aligned:
        w_all = w_all.transpose(0, 2, 1, 3)
    w_all = w_all.reshape(rows, model)
    w_in, w_down = w_all[: 2 * units], w_all[2 * units : 3 * units]

    last = (((1,), (1,)), ((), ()))
    first = (((0,), (0,)), ((), ()))
    pre = lax.dot_general(x_all, w_in, last, preferred_element_type=f32)
    grad_hidden = lax.dot_general(c_all, w_down, last, preferred_element_type=f32)
    gate_pre, up_pre = pre[:, :units], pre[:, units:]
    sigmoid_gate = jax.nn.sigmoid(gate_pre)
    activated = gate_pre * sigmoid_gate
    hidden = (activated * up_pre).astype(bf16)
    grad_gate = (
        grad_hidden * up_pre * sigmoid_gate * (1.0 + gate_pre * (1.0 - sigmoid_gate))
    ).astype(bf16)
    grad_up = (grad_hidden * activated).astype(bf16)
    grads = jnp.concatenate([grad_gate, grad_up], axis=1)
    g = jnp.concatenate(
        [
            lax.dot_general(grads, x_all, first, preferred_element_type=f32).astype(bf16),
            lax.dot_general(hidden, c_all, first, preferred_element_type=f32).astype(bf16),
            jnp.zeros((rows - 3 * units, model), bf16),
        ],
        axis=0,
    )
    g = g.reshape(w_shape if aligned else (n_rep, half, n_fs, depth))
    if not aligned:
        g = g.transpose(0, 2, 1, 3)
    n_sends = n_fs * (n_tp - 1) + 2 * n_fs * (n_rep - 1) + 3 * n_fs
    grad_inputs, dw = pl.pallas_call(
        functools.partial(scatter_kernel, (n_rep, n_fs, n_tp, n_y)),
        out_shape=(
            jax.ShapeDtypeStruct((tokens, width), bf16),
            jax.ShapeDtypeStruct((n_fs, n_rep, half, depth), bf16),
        ),
        in_specs=[VMEM] * 3,
        out_specs=(VMEM, ANY),
        scratch_shapes=[
            pltpu.VMEM((n_fs, tokens, model), bf16),
            pltpu.VMEM((n_tp - 1, n_fs, tokens, width), bf16),
            pltpu.VMEM((n_fs, tokens, width), bf16),
            pltpu.VMEM((n_y - 1, n_z, tokens, width), bf16),
            pltpu.VMEM((n_z, tokens, width), bf16),
            pltpu.VMEM((n_z, tokens, width), bf16),
            pltpu.VMEM((n_rep - 1, n_fs, half, depth), bf16),
            pltpu.VMEM((n_fs, half, depth), bf16),
            DMA((n_sends,)),
            DMA((n_tp - 1, n_fs)),
            DMA((n_y - 1, n_z)),
            DMA((n_z,)),
            DMA((n_rep - 1, n_fs)),
            DMA((n_rep, n_fs)),
        ],
        compiler_params=pltpu.CompilerParams(
            collective_id=1, has_side_effects=True, vmem_limit_bytes=60 * 2**20
        ),
    )(grads.reshape(n_fs, tokens, 2 * units), w_all, g)
    dw = dw.reshape(n_fs, rows, depth)
    gate_grads, up_grads, down_grads = (
        dw[:, i * units : (i + 1) * units].reshape(hidden_tp, depth) for i in range(3)
    )
    return (
        grad_inputs,
        gate_grads.T.astype(f32),
        up_grads.T.astype(f32),
        down_grads.astype(f32),
    )


def solution(mesh):
    n_rep, n_fs, n_tp = (mesh.shape[axis] for axis in ("rep", "fs", "tp"))
    placed = (
        P(("rep", "fs"), "tp"),
        P(("rep", "fs"), "tp"),
        P("fs", "tp"),
        P("fs", "tp"),
        P("tp", "fs"),
    )
    return jax.shard_map(
        functools.partial(per_device, n_rep, n_fs, n_tp),
        mesh=mesh,
        in_specs=placed,
        out_specs=(P(("rep", "fs"), "tp"), P("fs", "tp"), P("fs", "tp"), P("tp", "fs")),
        check_vma=False,
    )
```

profile of v0, /device:TPU:0, one launch (start us, length us, event | category | flops | bytes accessed | tf_op | source)
XLA Modules:
  0.0 169.0 jit_solution(2454043383256927473)
XLA Ops:
  0.6 0.1 pad.2.clone
  0.7 75.3 %shard_map.84 = (bf16[8,128,2048]{2,1,0:T(8,128)(2,1)}, bf16[8,128,2048]{2,1,0:T(8,128)(2,1)}, bf16[2,272,2048]{2,1,0:T(8,128)(2,1)}) custom-call(bf16[128,1024]{1,0:T(8,128)(2,1)} %x_ref.1, bf16[128,1024]{1,0:T(8,128)(2,1)} %c_ref.1, bf16[256,1408]{1,0:T(8,128)(2,1)} %refs_0_.1, bf16[256,1408]{1,0:T(8,128)(2,1)} %refs_1_.1, bf16[1408,256]{1,0:T(8,128)(2,1)} %refs_2_.1), custom_call_target="tpu_custom_call" | custom-call | tf_op jit(solution)/shard_map/pallas_call | solution.py:368
  76.0 0.0 copy-start.2
  76.0 4.5 %fusion = f32[1024,352]{0,1:T(8,128)S(1)} fusion(bf16[1024,2048]{1,0:T(8,128)(2,1)} %bitcast.29, bf16[544,2048]{1,0:T(8,128)(2,1)} %bitcast.25), kind=kOutput, calls=%fused_computation.3 | convolution fusion | flops 1476395008 | bytes 7077888 | tf_op jit(solution)/shard_map/dot_general | solution.py:388
  80.5 0.0 copy-done.2
  80.5 0.9 convolution_convert_fusion.1
  81.4 0.0 copy-start.1
  81.4 3.0 %multiply_convert_fusion.2 = (bf16[1024,176]{0,1:T(8,128)(2,1)S(1)}, bf16[1024,176]{0,1:T(8,128)(2,1)S(1)}) fusion(f32[1024,352]{0,1:T(8,128)S(1)} %fusion, bf16[1024,2048]{1,0:T(8,128)(2,1)S(1)} %bitcast.32, bf16[544,2048]{1,0:T(8,128)(2,1)} %bitcast.26), kind=kOutput, calls=%fused_computation.13 | convolution fusion | flops 740540416 | bytes 7077888 | tf_op jit(solution)/shard_map/dot_general | solution.py:389
  84.4 0.0 copy-done.1
  84.4 1.7 convolution_convert_fusion
  86.1 1.8 %maximum_maximum_fusion = bf16[544,2048]{1,0:T(8,128)(2,1)} fusion(bf16[176,2048]{1,0:T(8,128)(2,1)S(1)} %convolution_convert_fusion.1, bf16[352,2048]{1,0:T(8,128)(2,1)S(1)} %convolution_convert_fusion, bf16[544]{0:T(1024)(128)(2,1)S(1)} %pad.2.clone), kind=kLoop, calls=%fused_computation.2 | loop fusion | flops 6684672 | bytes 4392000 | tf_op jit(solution)/shard_map/concatenate | solution.py:399
  87.9 1.2 copy.12
  89.1 72.9 %shard_map.85 = (bf16[128,1024]{1,0:T(8,128)(2,1)}, bf16[8,2,272,256]{3,2,1,0:T(8,128)(2,1)}) custom-call(bf16[8,128,352]{2,1,0:T(8,128)(2,1)} %bitcast.24, bf16[544,2048]{1,0:T(8,128)(2,1)} %bitcast.27, bf16[2,272,2048]{2,1,0:T(8,128)(2,1)} %bitcast.23), custom_call_target="tpu_custom_call" | custom-call | tf_op jit(solution)/shard_map/pallas_call | solution.py:411
  162.0 1.7 %fusion.7 = (bf16[8,176,256]{2,1,0:T(8,128)(2,1)S(1)}, bf16[8,176,256]{2,1,0:T(8,128)(2,1)S(1)}, bf16[8,176,256]{2,1,0:T(8,128)(2,1)S(1)}) fusion(bf16[8,544,256]{2,1,0:T(8,128)(2,1)} %bitcast.28), kind=kLoop, calls=%fused_computation.17 | loop fusion | bytes 4325376 | tf_op jit(solution)/shard_map/slice | solution.py:441
  163.7 1.3 bitcast_convert_fusion
  164.9 0.3 convert_bitcast_fusion
  165.2 0.0 copy-start
  165.3 1.5 copy.14
  166.8 1.5 copy.13
  168.3 0.0 copy-done
  168.3 0.7 copy.16
  (2 shorter events, 0.1 us)
Async XLA Ops:
  76.0 4.5 %copy-start.2 = (bf16[8,128,2048]{2,1,0:T(8,128)(2,1)S(1)}, bf16[8,128,2048]{2,1,0:T(8,128)(2,1)}, u32[]{:S(2)}) copy-start(bf16[8,128,2048]{2,1,0:T(8,128)(2,1)} %get-tuple-element.9) | copy-start | bytes 12582916
  81.4 3.0 %copy-start.1 = (bf16[8,128,2048]{2,1,0:T(8,128)(2,1)S(1)}, bf16[8,128,2048]{2,1,0:T(8,128)(2,1)}, u32[]{:S(2)}) copy-start(bf16[8,128,2048]{2,1,0:T(8,128)(2,1)} %get-tuple-element.11) | copy-start | bytes 12582916
  165.2 3.1 %copy-start = (bf16[128,1024]{1,0:T(8,128)(2,1)S(1)}, bf16[128,1024]{1,0:T(8,128)(2,1)}, u32[]{:S(2)}) copy-start(bf16[128,1024]{1,0:T(8,128)(2,1)} %get-tuple-element.29) | copy-start | bytes 786436
where the time goes:
time: 169 us
  Pallas kernels  148 us (88%)
  matrix products  10 us (6%)
  local copies, waits for them, and re-layouts  6.71 us (4%)
  other arithmetic  3.41 us (2%)
    pallas_call x1, Pallas kernels, per_device(): pl.pallas_call(functools.partial(gather_kernel, (n_rep, n_fs, n_tp, n_y))...  75.3 us
    pallas_call x1, Pallas kernels, per_device(): pl.pallas_call(functools.partial(scatter_kernel, (n_rep, n_fs, n_tp, n_y)...  72.9 us
    dot_general x1, matrix products, per_device(): pre = lax.dot_general(x_all, w_in, last, preferred_element_type=f32)  4.46 us
    unnamed x9, local copies, waits for them, and re-layouts  3.79 us

commit v1 on v0

v1 whole, which is shorter than its diff:
```python
import functools

import jax
import jax.numpy as jnp
from jax import lax
from jax.experimental import pallas as pl
from jax.experimental.pallas import tpu as pltpu
from jax.sharding import PartitionSpec as P

MESH = pl.DeviceIdType.MESH


def enter(n_rep, n_fs, n_tp):
    barrier = pltpu.get_barrier_semaphore()
    for axis, n in (("rep", n_rep), ("fs", n_fs), ("tp", n_tp)):
        me = lax.axis_index(axis)
        for k in range(1, n):
            pl.semaphore_signal(
                barrier, inc=1, device_id={axis: lax.rem(me + k, n)}, device_id_type=MESH
            )
    pl.semaphore_wait(barrier, n_rep + n_fs + n_tp - 3)


class Sender:
    def __init__(self, sems):
        self.sems, self.used, self.pending = sems, 0, []

    def run(self, build, when):
        if when is None:
            build().start()
        else:
            pl.when(when)(lambda: build().start())

    def send(self, src, dst, recv_sem, axis, peer, when=None):
        def build(at=self.used):
            return pltpu.make_async_remote_copy(
                src_ref=src,
                dst_ref=dst,
                send_sem=self.sems.at[at],
                recv_sem=recv_sem,
                device_id={axis: peer},
                device_id_type=MESH,
            )

        self.used += 1
        self.run(build, when)
        self.pending.append((lambda: build().wait_send(), when))

    def local(self, src, dst):
        def build(at=self.used):
            return pltpu.make_async_copy(src, dst, self.sems.at[at])

        self.used += 1
        self.run(build, None)
        self.pending.append((lambda: build().wait(), None))

    def finish(self):
        for wait, when in self.pending:
            if when is None:
                wait()
            else:
                pl.when(when)(wait)


def arrived(slot, recv_sem, when=None):
    def wait():
        pltpu.make_async_copy(slot, slot, recv_sem).wait()

    if when is None:
        wait()
    else:
        pl.when(when)(wait)


def near_first(n):
    return sorted(range(1, n), key=lambda k: min(k, n - k))


def layer_kernel(
    sizes, x_ref, c_ref, gate_ref, up_ref, down_ref, dx_ref, dw_ref,
    xa, ca, wt, wa, pre, gt, ht, p, p_in, q, x_in, r, z_in, gp, go, g_in, gs,
    sends, act_recv, w_recv, p_recv, x_recv, z_recv, g_recv, d_recv,
):
    n_rep, n_fs, n_tp, n_y = sizes
    n_z = n_fs // n_y
    f32, bf16 = jnp.float32, jnp.bfloat16
    rep, fs, tp = (lax.axis_index(axis) for axis in ("rep", "fs", "tp"))
    z, y = fs // n_y, lax.rem(fs, n_y)
    tokens, width = x_ref.shape
    units, depth = wa.shape[1], down_ref.shape[1]
    group = n_z * tokens
    near = near_first(n_z)
    out = Sender(sends)
    enter(n_rep, n_fs, n_tp)

    def span(at, size):
        return pl.ds(pl.multiple_of(at * size, size), size)

    def peers(me, n):
        return [lax.rem(me + k, n) for k in range(1, n)]

    def at_z(other, row=y):
        return other * n_y + row

    own_acts, acts = (x_ref, c_ref), (xa, ca)

    def act_slot(a, shard, part):
        return acts[a].at[span(shard, tokens), span(part, width)]

    def act_send(a, shard, src, axis, peer, when=None):
        out.send(src, act_slot(a, shard, tp), act_recv.at[a, shard, tp], axis, peer, when)

    def to_rep(a, shard, src, when=None):
        for peer in peers(rep, n_rep):
            act_send(a, shard, src, "rep", peer, when)

    def to_tp(a, shard, src, when=None):
        for peer in peers(tp, n_tp):
            act_send(a, shard, src, "tp", peer, when)

    def from_rep(other):
        for peer in peers(rep, n_rep):
            for a in range(2):
                shard = peer * n_z + other
                slot = act_slot(a, shard, tp)
                arrived(slot, act_recv.at[a, shard, tp])
                to_tp(a, shard, slot)

    mine = rep * n_z + z
    for a in range(2):
        act_send(a, mine, own_acts[a], "fs", fs + n_y, z + 1 < n_z)
        act_send(a, mine, own_acts[a], "fs", fs - n_y, z >= 1)
        to_rep(a, mine, own_acts[a])
    for a in range(2):
        to_tp(a, mine, own_acts[a])

    wt[0] = gate_ref[...].T
    wt[1] = up_ref[...].T

    def w_part(i, owner):
        rows = span(owner, units)
        return down_ref.at[rows] if i == 2 else wt.at[i, rows]

    def w_slot(i, block):
        return wa.at[i, :, span(block, depth)]

    def w_send(i, block, src, peer):
        out.send(src, w_slot(i, block), w_recv.at[i, block], "fs", peer)

    for i in range(3):
        for row in peers(y, n_y):
            w_send(i, fs, w_part(i, mine), at_z(z, row))
    for i in range(3):
        wa[i, :, span(fs, depth)] = w_part(i, mine)[...]
    for a in range(2):
        acts[a][span(mine, tokens), span(tp, width)] = own_acts[a][...]

    def send_weights():
        for k in reversed(near):
            other = lax.rem(z + k, n_z)
            for i in range(3):
                w_send(i, fs, w_part(i, rep * n_z + other), at_z(other))

    for k in range(1, n_z):
        for a in range(2):
            for here, onward, step in ((z >= k, z + 1 < n_z, -1), (z + k < n_z, z >= 1, 1)):
                shard = mine + step * k
                slot = act_slot(a, shard, tp)
                arrived(slot, act_recv.at[a, shard, tp], here)
                if k < n_z - 1:
                    act_send(a, shard, slot, "fs", fs - step * n_y, jnp.logical_and(here, onward))
                to_rep(a, shard, slot, here)
                to_tp(a, shard, slot, here)
        if k == max(1, n_z - 2):
            send_weights()
        if k == 1:
            from_rep(z)
    if n_z == 1:
        from_rep(z)
    for k in near:
        other = lax.rem(z + n_z - k, n_z)
        for i in range(3):
            slot = w_slot(i, at_z(other))
            arrived(slot, w_recv.at[i, at_z(other)])
            for row in peers(y, n_y):
                w_send(i, at_z(other), slot, at_z(z, row))
        from_rep(other)
    for k in range(n_z):
        other = lax.rem(z + k, n_z)
        for i in range(3):
            for row in peers(y, n_y):
                arrived(w_slot(i, at_z(other, row)), w_recv.at[i, at_z(other, row)])
    for part in peers(tp, n_tp):
        for shard in range(n_rep * n_z):
            for a in range(2):
                arrived(act_slot(a, shard, part), act_recv.at[a, shard, part])

    last = (((1,), (1,)), ((), ()))
    first = (((0,), (0,)), ((), ()))

    def forward(side):
        cols = span(side, group)
        for i in range(3):
            pre[i] = lax.dot_general(
                wa[i], acts[i // 2][cols], last, preferred_element_type=f32
            )

        @pl.loop(0, units // 16)
        def _(step):
            rows, more = span(step, 16), pl.ds(pl.multiple_of(units + step * 16, 16), 16)
            gate_pre, up_pre, grad_hidden = pre[0, rows], pre[1, rows], pre[2, rows]
            sigmoid_gate = jax.nn.sigmoid(gate_pre)
            activated = gate_pre * sigmoid_gate
            ht[rows, cols] = (activated * up_pre).astype(bf16)
            gt[rows, cols] = (
                grad_hidden * up_pre * sigmoid_gate * (1.0 + gate_pre * (1.0 - sigmoid_gate))
            ).astype(bf16)
            gt[more, cols] = (grad_hidden * activated).astype(bf16)

    def partial_inputs(side):
        rows = span(side, group)
        w_in = wa[0:2].reshape(2 * units, wa.shape[2])
        p[rows] = lax.dot_general(gt[:, rows], w_in, first, preferred_element_type=f32).astype(bf16)
        for k in range(n_z):
            shard = side * n_z + lax.rem(z + k, n_z)
            for j in range(1, n_tp):
                peer = lax.rem(tp + j, n_tp)
                out.send(
                    p.at[span(shard, tokens), span(peer, width)],
                    p_in.at[j - 1, shard],
                    p_recv.at[j - 1, shard],
                    "tp",
                    peer,
                )

    def pair_sum(shard):
        total = p[span(shard, tokens), span(tp, width)].astype(f32)
        for j in range(n_tp - 1):
            arrived(p_in.at[j, shard], p_recv.at[j, shard])
            total = total + p_in[j, shard].astype(f32)
        return total

    def weight_block(block, dst):
        cols = span(block, depth)
        dst[0:2] = jnp.dot(gt[...], xa[:, cols], preferred_element_type=f32).astype(
            dst.dtype
        ).reshape(2, units, depth)
        dst[2] = jnp.dot(ht[...], ca[:, cols], preferred_element_type=f32).astype(dst.dtype)

    order = near + [0]
    for j in range(1, n_rep):
        side = lax.rem(rep + j, n_rep)
        forward(side)
        partial_inputs(side)
    forward(rep)
    for k in order:
        other = lax.rem(z + k, n_z)
        for j in range(1, n_rep):
            side = lax.rem(rep + j, n_rep)
            q[j - 1, other] = pair_sum(side * n_z + other).astype(bf16)
            out.send(
                q.at[j - 1, other], x_in.at[j - 1, other], x_recv.at[j - 1, other], "rep", side
            )
    for k in order:
        other = lax.rem(z + k, n_z)
        for j in range(1, n_y):
            row = lax.rem(y + j, n_y)
            weight_block(at_z(other, row), gp.at[j - 1, other])
            out.send(
                gp.at[j - 1, other], g_in.at[j - 1, other], g_recv.at[j - 1, other],
                "fs", at_z(z, row),
            )
    partial_inputs(rep)
    for k in order:
        other = lax.rem(z + k, n_z)
        weight_block(at_z(other), go.at[other])

    def dw_slot(side, other):
        return dw_ref.at[:, span(side * n_z + other, units)]

    def dw_send(other, src):
        for peer in peers(rep, n_rep):
            out.send(src, dw_slot(rep, other), d_recv.at[rep, other], "rep", peer)

    def x_step(k):
        other = lax.rem(z + k, n_z)
        total = pair_sum(mine - z + other)
        for j in range(n_rep - 1):
            arrived(x_in.at[j, other], x_recv.at[j, other])
            total = total + x_in[j, other].astype(f32)
        if k:
            r[other] = total.astype(bf16)
            out.send(r.at[other], z_in.at[z], z_recv.at[z], "fs", at_z(other))
        else:
            z_in[z] = total.astype(bf16)

    def g_step(k):
        other = lax.rem(z + k, n_z)
        total = go[other]
        for j in range(n_y - 1):
            arrived(g_in.at[j, other], g_recv.at[j, other])
            total = total + g_in[j, other].astype(f32)
        gs[other] = total.astype(bf16)
        if k:
            out.send(gs.at[other], dw_slot(rep, z), d_recv.at[rep, z], "fs", at_z(other))
        else:
            dw_send(z, gs.at[z])
            dw_ref[:, span(mine, units)] = gs[z]

    def g_forward(k):
        other = lax.rem(z + n_z - k, n_z)
        arrived(dw_slot(rep, other), d_recv.at[rep, other])
        dw_send(other, dw_slot(rep, other))

    for k in order:
        x_step(k)
        g_step(k)
    for k in near:
        g_forward(k)
    total = z_in[z].astype(f32)
    for k in near:
        other = lax.rem(z + n_z - k, n_z)
        arrived(z_in.at[other], z_recv.at[other])
        total = total + z_in[other].astype(f32)
    dx_ref[...] = total.astype(bf16)
    for side in peers(rep, n_rep):
        for k in range(n_z):
            other = lax.rem(z + n_z - k, n_z)
            arrived(dw_slot(side, other), d_recv.at[side, other])
    out.finish()


VMEM = pl.BlockSpec(memory_space=pltpu.VMEM)
DMA = pltpu.SemaphoreType.DMA


def fused(sizes, x, c, gate_weight, up_weight, down_weight):
    bf16, f32 = jnp.bfloat16, jnp.float32
    n_rep, n_fs, n_tp, n_y = sizes
    n_z = n_fs // n_y
    tokens, width = x.shape
    depth, hidden_tp = gate_weight.shape
    model, units = width * n_tp, hidden_tp // (n_rep * n_z)
    shards = n_rep * n_z
    group = shards * tokens
    grad_inputs, dw = pl.pallas_call(
        functools.partial(layer_kernel, sizes),
        out_shape=(
            jax.ShapeDtypeStruct((tokens, width), bf16),
            jax.ShapeDtypeStruct((3, hidden_tp, depth), bf16),
        ),
        in_specs=[VMEM] * 5,
        out_specs=(VMEM, VMEM),
        scratch_shapes=[
            pltpu.VMEM((group, model), bf16),
            pltpu.VMEM((group, model), bf16),
            pltpu.VMEM((2, hidden_tp, depth), bf16),
            pltpu.VMEM((3, units, model), bf16),
            pltpu.VMEM((3, units, n_z * tokens), f32),
            pltpu.VMEM((2 * units, group), bf16),
            pltpu.VMEM((units, group), bf16),
            pltpu.VMEM((group, model), bf16),
            pltpu.VMEM((n_tp - 1, shards, tokens, width), bf16),
            pltpu.VMEM((n_rep - 1, n_z, tokens, width), bf16),
            pltpu.VMEM((n_rep - 1, n_z, tokens, width), bf16),
            pltpu.VMEM((n_z, tokens, width), bf16),
            pltpu.VMEM((n_z, tokens, width), bf16),
            pltpu.VMEM((n_y - 1, n_z, 3, units, depth), bf16),
            pltpu.VMEM((n_z, 3, units, depth), f32),
            pltpu.VMEM((n_y - 1, n_z, 3, units, depth), bf16),
            pltpu.VMEM((n_z, 3, units, depth), bf16),
            DMA((256,)),
            DMA((2, shards, n_tp)),
            DMA((3, n_fs)),
            DMA((n_tp - 1, shards)),
            DMA((n_rep - 1, n_z)),
            DMA((n_z,)),
            DMA((n_y - 1, n_z)),
            DMA((n_rep, n_z)),
        ],
        compiler_params=pltpu.CompilerParams(
            collective_id=0, has_side_effects=True, vmem_limit_bytes=60 * 2**20
        ),
    )(x, c, gate_weight, up_weight, down_weight)
    return grad_inputs, dw[0].T.astype(f32), dw[1].T.astype(f32), dw[2].astype(f32)


def gathered(x, c, gate_weight, up_weight, down_weight):
    bf16, f32 = jnp.bfloat16, jnp.float32
    last = (((1,), (1,)), ((), ()))
    first = (((0,), (0,)), ((), ()))
    x, c = (lax.all_gather(v, "tp", axis=1, tiled=True) for v in (x, c))
    gate, up = (lax.all_gather(v, "fs", axis=0, tiled=True) for v in (gate_weight, up_weight))
    down = lax.all_gather(down_weight, "fs", axis=1, tiled=True)
    gate_pre = jnp.dot(x, gate, preferred_element_type=f32)
    up_pre = jnp.dot(x, up, preferred_element_type=f32)
    grad_hidden = lax.dot_general(c, down, last, preferred_element_type=f32)
    sigmoid_gate = jax.nn.sigmoid(gate_pre)
    activated = gate_pre * sigmoid_gate
    hidden = (activated * up_pre).astype(bf16)
    grad_gate = (
        grad_hidden * up_pre * sigmoid_gate * (1.0 + gate_pre * (1.0 - sigmoid_gate))
    ).astype(bf16)
    grad_up = (grad_hidden * activated).astype(bf16)
    partial_sum = lax.dot_general(grad_gate, gate, last, preferred_element_type=f32)
    partial_sum += lax.dot_general(grad_up, up, last, preferred_element_type=f32)
    grad_inputs = lax.psum_scatter(partial_sum, "tp", scatter_dimension=1, tiled=True)

    def scattered(lhs, rhs, dimension):
        grads = lax.dot_general(lhs, rhs, first, preferred_element_type=f32)
        grads = lax.psum_scatter(grads, "fs", scatter_dimension=dimension, tiled=True)
        return lax.psum(grads, "rep")

    return (
        grad_inputs.astype(bf16),
        scattered(x, grad_gate, 0),
        scattered(x, grad_up, 0),
        scattered(hidden, c, 1),
    )


def per_device(n_rep, n_fs, n_tp, x, c, gate_weight, up_weight, down_weight):
    n_y = max(k for k in range(1, n_fs + 1) if n_fs % k == 0 and k * k <= n_fs)
    n_z = n_fs // n_y
    tokens, width = x.shape
    depth, hidden_tp = gate_weight.shape
    args = (x, c, gate_weight, up_weight, down_weight)
    whole = hidden_tp % (16 * n_rep * n_z) == 0
    if whole and tokens % 128 == width % 128 == depth % 128 == 0 and min(n_rep, n_y, n_tp) > 1:
        return fused((n_rep, n_fs, n_tp, n_y), *args)
    return gathered(*args)


def solution(mesh):
    n_rep, n_fs, n_tp = (mesh.shape[axis] for axis in ("rep", "fs", "tp"))
    placed = (
        P(("rep", "fs"), "tp"),
        P(("rep", "fs"), "tp"),
        P("fs", "tp"),
        P("fs", "tp"),
        P("tp", "fs"),
    )
    return jax.shard_map(
        functools.partial(per_device, n_rep, n_fs, n_tp),
        mesh=mesh,
        in_specs=placed,
        out_specs=(P(("rep", "fs"), "tp"), P("fs", "tp"), P("fs", "tp"), P("tp", "fs")),
        check_vma=False,
    )
```

time: 169 us -> 155 us (0.917)
  matrix products: 10 us -> 0 us
  local copies, waits for them, and re-layouts: 6.71 us -> 3.78 us
    dot_general x4 -> x0, matrix products: 10 us -> none  [the longest x1 4.46 us: per_device(): pre = lax.dot_general(x_all, w_in, last, preferred_element_type=f32)]
    concatenate x2 -> x0, other arithmetic: 1.85 us -> none  [the longest x1 1.8 us: per_device(): jnp.concatenate([lax.dot_general(grads, x_all, first, preferred_element_t...]
    slice x1 -> x0, local copies, waits for them, and re-layouts: 1.69 us -> none  [per_device(): dw[:, i * units:(i + 1) * units].reshape(hidden_tp, depth)]
    pallas_call x2 -> x1, Pallas kernels: 148 us -> 148 us  [fused(): pl.pallas_call(functools.partial(layer_kernel, sizes), out_shape=(jax.Sha...]
    unnamed x9 -> x5, local copies, waits for them, and re-layouts: 3.79 us -> 3.78 us
where the time goes in v1:
time: 155 us
  Pallas kernels  148 us (95%)
  local copies, waits for them, and re-layouts  3.78 us (2%)
  other arithmetic  3 us (2%)
    pallas_call x1, Pallas kernels, fused(): pl.pallas_call(functools.partial(layer_kernel, sizes), out_shape=(jax.Sha...  148 us
    unnamed x5, local copies, waits for them, and re-layouts  3.78 us

profile of v1, /device:TPU:0, one launch (start us, length us, event | category | flops | bytes accessed | tf_op | source)
XLA Modules:
  0.0 155.0 jit_solution(5353623049429134890)
XLA Ops:
  0.6 147.6 %shard_map.84 = (bf16[128,1024]{1,0:T(8,128)(2,1)}, bf16[3,1408,256]{2,1,0:T(8,128)(2,1)}) custom-call(bf16[128,1024]{1,0:T(8,128)(2,1)} %x_ref.1, bf16[128,1024]{1,0:T(8,128)(2,1)} %c_ref.1, bf16[256,1408]{1,0:T(8,128)(2,1)} %gate_ref.1, bf16[256,1408]{1,0:T(8,128)(2,1)} %up_ref.1, bf16[1408,256]{1,0:T(8,128)(2,1)} %down_ref.1), custom_call_target="tpu_custom_call" | custom-call | tf_op jit(solution)/shard_map/pallas_call | solution.py:346
  148.3 3.0 %bitcast_convert_fusion = (f32[1408,256]{1,0:T(8,128)}, f32[256,1408]{0,1:T(8,128)S(1)}, f32[256,1408]{0,1:T(8,128)S(1)}) fusion(bf16[3,1408,256]{2,1,0:T(8,128)(2,1)} %get-tuple-element.7), kind=kLoop, calls=%fused_computation.2 | loop fusion | flops 1081344 | bytes 6488064 | tf_op jit(solution)/shard_map/convert_element_type | solution.py:385
  151.3 1.5 copy.10
  152.8 0.0 copy-start
  152.8 1.5 copy.9
  154.3 0.0 copy-done
  154.3 0.7 copy.12
Async XLA Ops:
  152.8 1.5 copy-start

commit v2 on v1

v2 whole, which is shorter than its diff:
```python
import functools

import jax
import jax.numpy as jnp
from jax import lax
from jax.experimental import pallas as pl
from jax.experimental.pallas import tpu as pltpu
from jax.sharding import PartitionSpec as P

MESH = pl.DeviceIdType.MESH


def greet(n_rep, n_fs, n_tp):
    barrier = pltpu.get_barrier_semaphore()
    for axis, n in (("rep", n_rep), ("fs", n_fs), ("tp", n_tp)):
        me = lax.axis_index(axis)
        for k in range(1, n):
            pl.semaphore_signal(
                barrier, inc=1, device_id={axis: lax.rem(me + k, n)}, device_id_type=MESH
            )
    return lambda: pl.semaphore_wait(barrier, n_rep + n_fs + n_tp - 3)


class Sender:
    def __init__(self, sems):
        self.sems, self.used, self.pending = sems, 0, []

    def run(self, build, when):
        if when is None:
            build().start()
        else:
            pl.when(when)(lambda: build().start())

    def send(self, src, dst, recv_sem, axis, peer, when=None):
        def build(at=self.used):
            return pltpu.make_async_remote_copy(
                src_ref=src,
                dst_ref=dst,
                send_sem=self.sems.at[at],
                recv_sem=recv_sem,
                device_id={axis: peer},
                device_id_type=MESH,
            )

        self.used += 1
        self.run(build, when)
        self.pending.append((lambda: build().wait_send(), when))

    def local(self, src, dst):
        def build(at=self.used):
            return pltpu.make_async_copy(src, dst, self.sems.at[at])

        self.used += 1
        self.run(build, None)
        self.pending.append((lambda: build().wait(), None))

    def finish(self):
        for wait, when in self.pending:
            if when is None:
                wait()
            else:
                pl.when(when)(wait)
        self.used, self.pending = 0, []


def arrived(slot, recv_sem, when=None):
    def wait():
        pltpu.make_async_copy(slot, slot, recv_sem).wait()

    if when is None:
        wait()
    else:
        pl.when(when)(wait)


def near_first(n):
    return sorted(range(1, n), key=lambda k: min(k, n - k))


def layer_kernel(
    sizes, *refs
):
    inputs, rest = refs[:5], refs[5:]
    outputs, local, loads, rest = rest[:4], rest[4:9], rest[9], rest[10:]
    met = greet(*sizes[:3])
    copies = [pltpu.make_async_copy(a, b, loads.at[i]) for i, (a, b) in enumerate(zip(inputs, local))]
    for copy in copies:
        copy.start()
    met()
    layer(sizes, copies, *local, *outputs, *rest)


def layer(
    sizes, copies, x_ref, c_ref, gate_ref, up_ref, down_ref, dx_ref, dgate_ref, dup_ref, ddown_ref,
    xa, ca, wt, wa, pre, pre_down, gt, ht, p, p_in, q, x_in, za, za_in, zb, zb_in, xz, xz_in,
    gp, go, g_in, gs, dw,
    sends, act_recv, w_recv, p_recv, x_recv, za_recv, zb_recv, xz_recv, g_recv, d_recv,
):
    n_rep, n_fs, n_tp, n_y = sizes
    n_z = n_fs // n_y
    f32, bf16 = jnp.float32, jnp.bfloat16
    rep, fs, tp = (lax.axis_index(axis) for axis in ("rep", "fs", "tp"))
    z, y = fs // n_y, lax.rem(fs, n_y)
    tokens, width = x_ref.shape
    units, depth = ht.shape[0], down_ref.shape[1]
    early = zb.shape[1]
    late = tokens - early
    out = Sender(sends)

    def span(at, size):
        return pl.ds(pl.multiple_of(at * size, size), size)

    def peers(me, n):
        return [lax.rem(me + k, n) for k in range(1, n)]

    def at_z(other, row=y):
        return other * n_y + row

    far_first, low, high = [], 0, n_z - 1
    for _ in range(n_z):
        above = high - z > z - low
        far_first.append(jnp.where(above, high, low))
        low, high = jnp.where(above, low, low + 1), jnp.where(above, high - 1, high)
    others = far_first[:-1]
    near = [z] + others[::-1]

    own_acts, acts = (x_ref, c_ref), (xa, ca)

    def act_slot(a, shard, part):
        return acts[a].at[span(shard, tokens), span(part, width)]

    def act_send(a, shard, src, axis, peer, when=None):
        out.send(src, act_slot(a, shard, tp), act_recv.at[a, shard, tp], axis, peer, when)

    def to_rep(a, shard, src, when=None):
        for peer in peers(rep, n_rep):
            act_send(a, shard, src, "rep", peer, when)

    def to_tp(a, shard, src, when=None):
        for peer in peers(tp, n_tp):
            act_send(a, shard, src, "tp", peer, when)

    def from_rep(other):
        for peer in peers(rep, n_rep):
            for a in range(2):
                shard = peer * n_z + other
                slot = act_slot(a, shard, tp)
                arrived(slot, act_recv.at[a, shard, tp])
                to_tp(a, shard, slot)

    mine = rep * n_z + z
    for a in range(2):
        copies[a].wait()
        act_send(a, mine, own_acts[a], "fs", fs + n_y, z + 1 < n_z)
        act_send(a, mine, own_acts[a], "fs", fs - n_y, z >= 1)
        to_rep(a, mine, own_acts[a])
    for a in range(2):
        to_tp(a, mine, own_acts[a])

    for copy in copies[2:]:
        copy.wait()
    wt[0] = gate_ref[...].T
    wt[1] = up_ref[...].T

    def w_part(i, owner):
        rows = span(owner, units)
        return down_ref.at[rows] if i == 2 else wt.at[i, rows]

    def w_slot(i, block):
        return wa.at[pl.ds(i * units, units), span(block, depth)]

    def w_send(i, block, src, peer, when=None):
        out.send(src, w_slot(i, block), w_recv.at[i, block], "fs", peer, when)

    for i in range(3):
        for row in peers(y, n_y):
            w_send(i, fs, w_part(i, mine), at_z(z, row))
    for i in range(3):
        wa[i * units : (i + 1) * units, span(fs, depth)] = w_part(i, mine)[...]
    for a in range(2):
        acts[a][span(mine, tokens), span(tp, width)] = own_acts[a][...]

    def send_weights(steps):
        for step in steps:
            for sign, here in ((1, z + step < n_z), (-1, z >= step)):
                other = z + sign * step
                for i in range(3):
                    w_send(i, fs, w_part(i, rep * n_z + other), at_z(other), here)

    def swap_weights(other):
        for i in range(3):
            slot = w_slot(i, at_z(other))
            arrived(slot, w_recv.at[i, at_z(other)])
            for row in peers(y, n_y):
                w_send(i, at_z(other), slot, at_z(z, row))

    swapped = 1
    for k in range(1, n_z):
        for a in range(2):
            for here, onward, step in ((z >= k, z + 1 < n_z, -1), (z + k < n_z, z >= 1, 1)):
                shard = mine + step * k
                slot = act_slot(a, shard, tp)
                arrived(slot, act_recv.at[a, shard, tp], here)
                if k < n_z - 1:
                    act_send(a, shard, slot, "fs", fs - step * n_y, jnp.logical_and(here, onward))
                to_rep(a, shard, slot, here)
                to_tp(a, shard, slot, here)
            if k < n_z - 1:
                continue
            if a == 0:
                send_weights([k])
            if swapped < k:
                swap_weights(near[swapped])
                swapped += 1
        if k < n_z - 1:
            send_weights([k])
        if k == 1:
            from_rep(z)
        if 1 < k == n_z - 2:
            swap_weights(near[1])
            swapped = 2
    if n_z == 1:
        from_rep(z)
    for k in range(swapped, n_z):
        swap_weights(near[k])
    for k in range(1, n_z):
        from_rep(near[k])
    for part in peers(tp, n_tp):
        for shard in range(n_rep * n_z):
            for a in range(2):
                arrived(act_slot(a, shard, part), act_recv.at[a, shard, part])

    last = (((1,), (1,)), ((), ()))
    first = (((0,), (0,)), ((), ()))

    def contract(block, fresh):
        cols = span(block, depth)
        for ref, rows, act in ((pre, slice(0, 2 * units), xa), (pre_down, slice(2 * units, 3 * units), ca)):
            part = lax.dot_general(wa[rows, cols], act[:, cols], last, preferred_element_type=f32)
            ref[...] = part if fresh else ref[...] + part

    for k in range(n_z):
        contract(at_z(near[k]), k == 0)
        for row in peers(y, n_y):
            for i in range(3):
                arrived(w_slot(i, at_z(near[k], row)), w_recv.at[i, at_z(near[k], row)])
            contract(at_z(near[k], row), False)

    out.finish()

    def activate(side):
        cols = span(side, n_z * tokens)

        @pl.loop(0, units // 16)
        def _(step):
            rows, more = span(step, 16), pl.ds(pl.multiple_of(units + step * 16, 16), 16)
            gate_pre, up_pre, grad_hidden = pre[rows, cols], pre[more, cols], pre_down[rows, cols]
            sigmoid_gate = jax.nn.sigmoid(gate_pre)
            activated = gate_pre * sigmoid_gate
            ht[rows, cols] = (activated * up_pre).astype(bf16)
            gt[rows, cols] = (
                grad_hidden * up_pre * sigmoid_gate * (1.0 + gate_pre * (1.0 - sigmoid_gate))
            ).astype(bf16)
            gt[more, cols] = (grad_hidden * activated).astype(bf16)

    def partial_inputs(side):
        rows = span(side, n_z * tokens)
        p[rows] = lax.dot_general(
            gt[:, rows], wa[: 2 * units], first, preferred_element_type=f32
        ).astype(bf16)
        for other in far_first:
            shard = side * n_z + other
            for j in range(1, n_tp):
                peer = lax.rem(tp + j, n_tp)
                out.send(
                    p.at[span(shard, tokens), span(peer, width)],
                    p_in.at[j - 1, shard],
                    p_recv.at[j - 1, shard],
                    "tp",
                    peer,
                )

    def pair_wait(shard):
        for j in range(n_tp - 1):
            arrived(p_in.at[j, shard], p_recv.at[j, shard])

    def pair_sum(shard, low, size):
        rows = pl.ds(pl.multiple_of(shard * tokens + low, 16), size)
        total = p[rows, span(tp, width)].astype(f32)
        for j in range(n_tp - 1):
            total = total + p_in[j, shard, low : low + size].astype(f32)
        return total

    def weight_block(block, dst):
        cols = span(block, depth)
        dst[: 2 * units] = jnp.dot(gt[...], xa[:, cols], preferred_element_type=f32).astype(
            dst.dtype
        )
        dst[2 * units :] = jnp.dot(ht[...], ca[:, cols], preferred_element_type=f32).astype(
            dst.dtype
        )

    def chain(value, buf, box, box_recv, other, inner):
        up = other > z
        came = jnp.where(up, 0, 1)
        behind = jnp.where(up, z >= 1, z + 1 < n_z)

        @pl.when(behind if inner else jnp.logical_not(behind))
        def _():
            for low, size, total in value(other):
                rows = pl.ds(low, size)
                if inner:
                    if low == 0:
                        arrived(box.at[came, other], box_recv.at[came, other])
                    total = total + box[came, other, rows].astype(f32)
                buf[other, rows] = total.astype(bf16)

        if inner:
            out.send(
                buf.at[other], box.at[came, other], box_recv.at[came, other],
                "fs", jnp.where(up, fs + n_y, fs - n_y), behind,
            )
        else:
            out.send(
                buf.at[other], box.at[came, other], box_recv.at[came, other],
                "fs", jnp.where(up, fs + n_y, fs - n_y), jnp.logical_not(behind),
            )

    def chain_end(value, acc, box, box_recv):
        for low, size, total in value(z):
            acc[pl.ds(low, size)] = total
        for came, here in ((0, z >= 1), (1, z + 1 < n_z)):

            @pl.when(here)
            def _():
                arrived(box.at[came, z], box_recv.at[came, z])
                acc[...] = acc[...] + box[came, z].astype(f32)

    def late_rows(other):
        return [
            (side * late, late, pair_sum(side * n_z + other, early, late)) for side in range(n_rep)
        ]

    def early_rows(other):
        total = pair_sum(rep * n_z + other, 0, early)
        for j in range(n_rep - 1):
            total = total + x_in[j, other].astype(f32)
        return [(0, early, total)]

    def x_arrived(other):
        for j in range(n_rep - 1):
            arrived(x_in.at[j, other], x_recv.at[j, other])

    def dw_slot(side, other):
        return dw.at[side * n_z + other]

    def dw_send(other, src):
        for peer in peers(rep, n_rep):
            out.send(src, dw_slot(rep, other), d_recv.at[rep, other], "rep", peer)

    def g_step(other, mine_too):
        total = go[other]
        for j in range(n_y - 1):
            arrived(g_in.at[j, other], g_recv.at[j, other])
            total = total + g_in[j, other].astype(f32)
        if mine_too:
            dw[mine] = total.astype(bf16)
            dw_send(z, dw_slot(rep, z))
        else:
            gs[other] = total.astype(bf16)
            out.send(gs.at[other], dw_slot(rep, z), d_recv.at[rep, z], "fs", at_z(other))

    def g_forward(other):
        arrived(dw_slot(rep, other), d_recv.at[rep, other])
        dw_send(other, dw_slot(rep, other))

    def to_row(other):
        for j in range(1, n_y):
            row = lax.rem(y + j, n_y)
            weight_block(at_z(other, row), gp.at[j - 1, other])
            out.send(
                gp.at[j - 1, other], g_in.at[j - 1, other], g_recv.at[j - 1, other],
                "fs", at_z(z, row),
            )

    def to_side(other):
        for j in range(1, n_rep):
            side = lax.rem(rep + j, n_rep)
            pair_wait(side * n_z + other)
            q[j - 1, other] = pair_sum(side * n_z + other, 0, early).astype(bf16)
            out.send(
                q.at[j - 1, other], x_in.at[j - 1, other], x_recv.at[j - 1, other], "rep", side
            )

    for j in range(1, n_rep):
        side = lax.rem(rep + j, n_rep)
        activate(side)
        partial_inputs(side)
    activate(rep)
    to_row(z)
    for other in far_first:
        to_side(other)
    partial_inputs(rep)
    for other in others:
        to_row(other)
    for other in far_first:
        pair_wait(rep * n_z + other)
    for other in others:
        chain(late_rows, za, za_in, za_recv, other, False)
    for other in [z] + others:
        weight_block(at_z(other), go.at[other])
    def late_on(other):
        chain(late_rows, za, za_in, za_recv, other, True)

    g_step(z, True)
    for i, other in enumerate(others):
        g_step(other, False)
        x_arrived(other)
        chain(early_rows, zb, zb_in, zb_recv, other, False)
        if i:
            late_on(others[i - 1])
    if others:
        late_on(others[-1])
    chain_end(late_rows, xz.at[0, : n_rep * late], za_in, za_recv)
    for j in range(1, n_rep):
        side = lax.rem(rep + j, n_rep)
        xz_in[j - 1, 0] = xz[0, span(side, late)].astype(bf16)
        out.send(xz_in.at[j - 1, 0], xz_in.at[j - 1, 1], xz_recv.at[j - 1], "rep", side)
    for other in others:
        g_forward(other)
        chain(early_rows, zb, zb_in, zb_recv, other, True)
    x_arrived(z)
    chain_end(early_rows, xz.at[1, :early], zb_in, zb_recv)
    dx_ref[:early] = xz[1, :early].astype(bf16)
    total = xz[0, span(rep, late)]
    for j in range(n_rep - 1):
        arrived(xz_in.at[j, 1], xz_recv.at[j])
        total = total + xz_in[j, 1].astype(f32)
    dx_ref[early:] = total.astype(bf16)
    for side in peers(rep, n_rep):
        for other in [z] + others:
            arrived(dw_slot(side, other), d_recv.at[side, other])
    whole = dw[...]
    dgate_ref[...] = whole[:, :units].reshape(dgate_ref.shape[::-1]).T
    dup_ref[...] = whole[:, units : 2 * units].reshape(dup_ref.shape[::-1]).T
    ddown_ref[...] = whole[:, 2 * units :].reshape(ddown_ref.shape)
    out.finish()


VMEM = pl.BlockSpec(memory_space=pltpu.VMEM)
ANY = pl.BlockSpec(memory_space=pl.ANY)
DMA = pltpu.SemaphoreType.DMA


def fused(sizes, x, c, gate_weight, up_weight, down_weight):
    bf16, f32 = jnp.bfloat16, jnp.float32
    n_rep, n_fs, n_tp, n_y = sizes
    n_z = n_fs // n_y
    tokens, width = x.shape
    depth, hidden_tp = gate_weight.shape
    model, units = width * n_tp, hidden_tp // (n_rep * n_z)
    shards = n_rep * n_z
    group = shards * tokens
    tp_rep = n_tp + n_rep - 2
    n_sends = (
        2 * (2 + tp_rep) + 4 * ((n_z - 1) * (1 + tp_rep) - 1) + 2 * n_z * (n_rep - 1) * (n_tp - 1)
        + 3 * (n_y - 1) * n_z + 6 * (n_z - 1)
    )
    late = tokens * 3 // 128 * 16
    early = tokens - late
    grad_inputs, *grads = pl.pallas_call(
        functools.partial(layer_kernel, sizes),
        out_shape=(
            jax.ShapeDtypeStruct((tokens, width), bf16),
            jax.ShapeDtypeStruct((depth, hidden_tp), bf16),
            jax.ShapeDtypeStruct((depth, hidden_tp), bf16),
            jax.ShapeDtypeStruct((hidden_tp, depth), bf16),
        ),
        in_specs=[ANY] * 5,
        out_specs=(VMEM,) * 4,
        scratch_shapes=[
            *(pltpu.VMEM(v.shape, bf16) for v in (x, c, gate_weight, up_weight, down_weight)),
            DMA((5,)),
            pltpu.VMEM((group, model), bf16),
            pltpu.VMEM((group, model), bf16),
            pltpu.VMEM((2, hidden_tp, depth), bf16),
            pltpu.VMEM((3 * units, model), bf16),
            pltpu.VMEM((2 * units, group), f32),
            pltpu.VMEM((units, group), f32),
            pltpu.VMEM((2 * units, group), bf16),
            pltpu.VMEM((units, group), bf16),
            pltpu.VMEM((group, model), bf16),
            pltpu.VMEM((n_tp - 1, shards, tokens, width), bf16),
            pltpu.VMEM((n_rep - 1, n_z, early, width), bf16),
            pltpu.VMEM((n_rep - 1, n_z, early, width), bf16),
            pltpu.VMEM((n_z, n_rep * late, width), bf16),
            pltpu.VMEM((2, n_z, n_rep * late, width), bf16),
            pltpu.VMEM((n_z, early, width), bf16),
            pltpu.VMEM((2, n_z, early, width), bf16),
            pltpu.VMEM((2, max(early, n_rep * late), width), f32),
            pltpu.VMEM((n_rep - 1, 2, late, width), bf16),
            pltpu.VMEM((n_y - 1, n_z, 3 * units, depth), bf16),
            pltpu.VMEM((n_z, 3 * units, depth), f32),
            pltpu.VMEM((n_y - 1, n_z, 3 * units, depth), bf16),
            pltpu.VMEM((n_z, 3 * units, depth), bf16),
            pltpu.VMEM((shards, 3 * units, depth), bf16),
            DMA((n_sends,)),
            DMA((2, shards, n_tp)),
            DMA((3, n_fs)),
            DMA((n_tp - 1, shards)),
            DMA((n_rep - 1, n_z)),
            DMA((2, n_z)),
            DMA((2, n_z)),
            DMA((n_rep - 1,)),
            DMA((n_y - 1, n_z)),
            DMA((n_rep, n_z)),
        ],
        compiler_params=pltpu.CompilerParams(
            collective_id=0, has_side_effects=True, vmem_limit_bytes=60 * 2**20
        ),
    )(x, c, gate_weight, up_weight, down_weight)
    return grad_inputs, *(v.astype(f32) for v in grads)


def gathered(x, c, gate_weight, up_weight, down_weight):
    bf16, f32 = jnp.bfloat16, jnp.float32
    last = (((1,), (1,)), ((), ()))
    first = (((0,), (0,)), ((), ()))
    x, c = (lax.all_gather(v, "tp", axis=1, tiled=True) for v in (x, c))
    gate, up = (lax.all_gather(v, "fs", axis=0, tiled=True) for v in (gate_weight, up_weight))
    down = lax.all_gather(down_weight, "fs", axis=1, tiled=True)
    gate_pre = jnp.dot(x, gate, preferred_element_type=f32)
    up_pre = jnp.dot(x, up, preferred_element_type=f32)
    grad_hidden = lax.dot_general(c, down, last, preferred_element_type=f32)
    sigmoid_gate = jax.nn.sigmoid(gate_pre)
    activated = gate_pre * sigmoid_gate
    hidden = (activated * up_pre).astype(bf16)
    grad_gate = (
        grad_hidden * up_pre * sigmoid_gate * (1.0 + gate_pre * (1.0 - sigmoid_gate))
    ).astype(bf16)
    grad_up = (grad_hidden * activated).astype(bf16)
    partial_sum = lax.dot_general(grad_gate, gate, last, preferred_element_type=f32)
    partial_sum += lax.dot_general(grad_up, up, last, preferred_element_type=f32)
    grad_inputs = lax.psum_scatter(partial_sum, "tp", scatter_dimension=1, tiled=True)

    def scattered(lhs, rhs, dimension):
        grads = lax.dot_general(lhs, rhs, first, preferred_element_type=f32)
        grads = lax.psum_scatter(grads, "fs", scatter_dimension=dimension, tiled=True)
        return lax.psum(grads, "rep")

    return (
        grad_inputs.astype(bf16),
        scattered(x, grad_gate, 0),
        scattered(x, grad_up, 0),
        scattered(hidden, c, 1),
    )


def per_device(n_rep, n_fs, n_tp, x, c, gate_weight, up_weight, down_weight):
    n_y = max(k for k in range(1, n_fs + 1) if n_fs % k == 0 and k * k <= n_fs)
    n_z = n_fs // n_y
    tokens, width = x.shape
    depth, hidden_tp = gate_weight.shape
    args = (x, c, gate_weight, up_weight, down_weight)
    whole = hidden_tp % (16 * n_rep * n_z) == 0
    if whole and tokens % 128 == width % 128 == depth % 128 == 0 and min(n_rep, n_y, n_tp) > 1:
        return fused((n_rep, n_fs, n_tp, n_y), *args)
    return gathered(*args)


def solution(mesh):
    n_rep, n_fs, n_tp = (mesh.shape[axis] for axis in ("rep", "fs", "tp"))
    placed = (
        P(("rep", "fs"), "tp"),
        P(("rep", "fs"), "tp"),
        P("fs", "tp"),
        P("fs", "tp"),
        P("tp", "fs"),
    )
    return jax.shard_map(
        functools.partial(per_device, n_rep, n_fs, n_tp),
        mesh=mesh,
        in_specs=placed,
        out_specs=(P(("rep", "fs"), "tp"), P("fs", "tp"), P("fs", "tp"), P("tp", "fs")),
        check_vma=False,
    )
```

time: 155 us -> 140 us (0.903)
  the two profiles are of different devices: /device:TPU:0 before, /device:TPU:16 now
where the time goes in v2:
time: 140 us
  Pallas kernels  134 us (96%)
  other arithmetic  4.77 us (3%)
    pallas_call x1, Pallas kernels, fused(): pl.pallas_call(functools.partial(layer_kernel, sizes), out_shape=(jax.Sha...  134 us
    convert_element_type x3, other arithmetic, fused(): return (grad_inputs, *(v.astype(f32) for v in grads))  4.77 us

profile of v2, /device:TPU:16, one launch (start us, length us, event | category | flops | bytes accessed | tf_op | source)
XLA Modules:
  0.0 140.1 jit_solution(1595776941532476883)
XLA Ops:
  0.6 133.8 %shard_map.84 = (bf16[128,1024]{1,0:T(8,128)(2,1)}, bf16[256,1408]{1,0:T(8,128)(2,1)}, bf16[256,1408]{1,0:T(8,128)(2,1)}, bf16[1408,256]{1,0:T(8,128)(2,1)}) custom-call(bf16[128,1024]{1,0:T(8,128)(2,1)} %refs_0_.1, bf16[128,1024]{1,0:T(8,128)(2,1)} %refs_1_.1, bf16[256,1408]{1,0:T(8,128)(2,1)} %refs_2_.1, bf16[256,1408]{1,0:T(8,128)(2,1)} %refs_3_.1, ...), custom_call_target="tpu_custom_call" | custom-call | tf_op jit(solution)/shard_map/pallas_call | solution.py:471
  134.4 0.0 copy-start.1
  134.4 2.4 %convert_element_type.9 = f32[256,1408]{1,0:T(8,128)} convert(bf16[256,1408]{1,0:T(8,128)(2,1)} %get-tuple-element.9) | non-fusion elementwise | flops 360448 | bytes 2162688 | tf_op jit(solution)/shard_map/convert_element_type | solution.py:522
  136.8 0.0 copy-done.1
  136.8 0.0 copy-start
  136.8 1.2 convert_element_type.10
  138.0 0.2 copy-done
  138.2 0.0 copy-start.2
  138.2 1.2 convert_element_type.11
  139.4 0.0 copy-done.2
  139.4 0.7 copy.10
Async XLA Ops:
  134.4 2.4 %copy-start.1 = (bf16[256,1408]{1,0:T(8,128)(2,1)S(1)}, bf16[256,1408]{1,0:T(8,128)(2,1)}, u32[]{:S(2)}) copy-start(bf16[256,1408]{1,0:T(8,128)(2,1)} %get-tuple-element.10) | copy-start | bytes 2162692
  136.8 1.4 copy-start
  138.2 1.2 copy-start.2

commit v3 on v2

v3 whole, which is shorter than its diff:
```python
import functools

import jax
import jax.numpy as jnp
from jax import lax
from jax.experimental import pallas as pl
from jax.experimental.pallas import tpu as pltpu
from jax.sharding import PartitionSpec as P

MESH = pl.DeviceIdType.MESH


def greet(n_rep, n_fs, n_tp):
    barrier = pltpu.get_barrier_semaphore()
    for axis, n in (("rep", n_rep), ("fs", n_fs), ("tp", n_tp)):
        me = lax.axis_index(axis)
        for k in range(1, n):
            pl.semaphore_signal(
                barrier, inc=1, device_id={axis: lax.rem(me + k, n)}, device_id_type=MESH
            )
    return lambda: pl.semaphore_wait(barrier, n_rep + n_fs + n_tp - 3)


class Sender:
    def __init__(self, sems):
        self.sems, self.used, self.pending = sems, 0, []

    def run(self, build, when):
        if when is None:
            build().start()
        else:
            pl.when(when)(lambda: build().start())

    def send(self, src, dst, recv_sem, axis, peer, when=None):
        def build(at=self.used):
            return pltpu.make_async_remote_copy(
                src_ref=src,
                dst_ref=dst,
                send_sem=self.sems.at[at],
                recv_sem=recv_sem,
                device_id={axis: peer},
                device_id_type=MESH,
            )

        self.used += 1
        self.run(build, when)
        self.pending.append((lambda: build().wait_send(), when))

    def local(self, src, dst):
        def build(at=self.used):
            return pltpu.make_async_copy(src, dst, self.sems.at[at])

        self.used += 1
        self.run(build, None)
        self.pending.append((lambda: build().wait(), None))

    def finish(self):
        for wait, when in self.pending:
            if when is None:
                wait()
            else:
                pl.when(when)(wait)
        self.used, self.pending = 0, []


def arrived(slot, recv_sem, when=None):
    def wait():
        pltpu.make_async_copy(slot, slot, recv_sem).wait()

    if when is None:
        wait()
    else:
        pl.when(when)(wait)


def near_first(n):
    return sorted(range(1, n), key=lambda k: min(k, n - k))


def layer_kernel(
    sizes, *refs
):
    inputs, rest = refs[:5], refs[5:]
    outputs, local, loads, rest = rest[:4], rest[4:9], rest[9], rest[10:]
    met = greet(*sizes[:3])
    copies = [pltpu.make_async_copy(a, b, loads.at[i]) for i, (a, b) in enumerate(zip(inputs, local))]
    for copy in copies:
        copy.start()
    met()
    layer(sizes, copies, *local, *outputs, *rest)


def layer(
    sizes, copies, x_ref, c_ref, gate_ref, up_ref, down_ref, dx_ref, dgate_ref, dup_ref, ddown_ref,
    xa, ca, wt, wa, wa_more, pre, pre_down, gt, ht,
    p, p_in, q, x_in, r, z_in, total,
    gp, go, g_in, gs, dw, gp_more, go_more, g_in_more, gs_more, dw_more,
    sends, act_recv, w_recv, p_recv, x_recv, z_recv, g_recv, d_recv,
):
    n_rep, n_fs, n_tp, n_y = sizes
    n_z = n_fs // n_y
    f32, bf16 = jnp.float32, jnp.bfloat16
    rep, fs, tp = (lax.axis_index(axis) for axis in ("rep", "fs", "tp"))
    z, y = fs // n_y, lax.rem(fs, n_y)
    tokens, width = x_ref.shape
    base, more, depth = wa.shape[1], ht.shape[0] - wa.shape[1], down_ref.shape[1]
    units = base + more
    inner = jnp.logical_and(z > 0, z < n_z - 1) if more else None
    out = Sender(sends)

    def span(at, size):
        return pl.ds(pl.multiple_of(at * size, size), size)

    def peers(me, n):
        return [lax.rem(me + k, n) for k in range(1, n)]

    def at_z(other, row=y):
        return other * n_y + row

    far_first, low, high = [], 0, n_z - 1
    for _ in range(n_z):
        above = 2 * (high - z) + jnp.where(2 * z < n_z, 1, 0) > 2 * (z - low)
        far_first.append(jnp.where(above, high, low))
        low, high = jnp.where(above, low, low + 1), jnp.where(above, high - 1, high)
    others = far_first[:-1]
    near = [z] + others[::-1]

    own_acts, acts = (x_ref, c_ref), (xa, ca)

    def act_slot(a, shard, part):
        return acts[a].at[span(shard, tokens), span(part, width)]

    def act_send(a, shard, src, axis, peer, when=None):
        out.send(src, act_slot(a, shard, tp), act_recv.at[a, shard, tp], axis, peer, when)

    def to_rep(a, shard, src, when=None):
        for peer in peers(rep, n_rep):
            act_send(a, shard, src, "rep", peer, when)

    def to_tp(a, shard, src, when=None):
        for peer in peers(tp, n_tp):
            act_send(a, shard, src, "tp", peer, when)

    def from_rep(other):
        for peer in peers(rep, n_rep):
            for a in range(2):
                shard = peer * n_z + other
                slot = act_slot(a, shard, tp)
                arrived(slot, act_recv.at[a, shard, tp])
                to_tp(a, shard, slot)

    mine = rep * n_z + z
    for a in range(2):
        copies[a].wait()
        act_send(a, mine, own_acts[a], "fs", fs + n_y, z + 1 < n_z)
        act_send(a, mine, own_acts[a], "fs", fs - n_y, z >= 1)
        to_rep(a, mine, own_acts[a])
    for a in range(2):
        to_tp(a, mine, own_acts[a])

    for copy in copies[2:]:
        copy.wait()
    wt[0] = gate_ref[...].T
    wt[1] = up_ref[...].T

    def inside(other):
        return jnp.logical_and(other > 0, other < n_z - 1)

    parts = [(0, 0), (0, 1), (1, 0), (1, 1)][: 4 if more else 2]
    here_too = {0: None, 1: inner}

    def w_part(extra, kind, other):
        start = rep * (n_z * base + max(n_z - 2, 0) * more) + other * units
        start = start - (jnp.minimum(other, 1) * more if more else 0) + extra * base
        rows = pl.ds(pl.multiple_of(start, 16), more if extra else base)
        return down_ref.at[rows] if kind else wt.at[:, rows]

    def w_slot(extra, kind, block):
        held = wa_more if extra else wa
        return held.at[2 if kind else slice(0, 2), :, span(block, depth)]

    def w_send(part, block, src, peer, when=None):
        out.send(src, w_slot(*part, block), w_recv.at[parts.index(part), block], "fs", peer, when)

    def w_arrived(part, block):
        arrived(w_slot(*part, block), w_recv.at[parts.index(part), block], here_too[part[0]])

    for part in parts:
        for row in peers(y, n_y):
            w_send(part, fs, w_part(*part, z), at_z(z, row), here_too[part[0]])

    def keep(part):
        held, (extra, kind) = (wa_more if part[0] else wa), part
        if kind:
            held[2, :, span(fs, depth)] = w_part(*part, z)[...]
        else:
            held[0:2, :, span(fs, depth)] = w_part(*part, z)[...]

    for part in parts:
        if part[0]:
            pl.when(inner)(functools.partial(keep, part))
        else:
            keep(part)
    for a in range(2):
        acts[a][span(mine, tokens), span(tp, width)] = own_acts[a][...]

    def send_weights(step, only=None):
        for sign, here in ((1, z + step < n_z), (-1, z >= step)):
            other = z + sign * step
            here = here if only is None else jnp.logical_and(here, only)
            for part in parts:
                when = jnp.logical_and(here, inside(other)) if part[0] else here
                w_send(part, fs, w_part(*part, other), at_z(other), when)

    def swap_weights(other):
        for part in parts:
            block = at_z(other)
            w_arrived(part, block)
            for row in peers(y, n_y):
                w_send(part, block, w_slot(*part, block), at_z(z, row), here_too[part[0]])

    held = n_z > 3
    for k in range(1, n_z):
        for a in range(2):
            for here, onward, step in ((z >= k, z + 1 < n_z, -1), (z + k < n_z, z >= 1, 1)):
                shard = mine + step * k
                slot = act_slot(a, shard, tp)
                arrived(slot, act_recv.at[a, shard, tp], here)
                if k < n_z - 1:
                    act_send(a, shard, slot, "fs", fs - step * n_y, jnp.logical_and(here, onward))
                to_rep(a, shard, slot, here)
                to_tp(a, shard, slot, here)
            if k == n_z - 1 and a == 0:
                send_weights(k)
        if k < n_z - 2 or not held and k == n_z - 2:
            send_weights(k)
        if k == 1:
            from_rep(z)
        if held and k == n_z - 2:
            send_weights(k, jnp.logical_not(inside(z)))
            swap_weights(near[1])
    if n_z == 1:
        from_rep(z)
    if held:
        swap_weights(near[2])
        send_weights(n_z - 2, inside(z))
    for k in range(3 if held else 1, n_z):
        swap_weights(near[k])
    for k in range(1, n_z):
        from_rep(near[k])
    for part in peers(tp, n_tp):
        for shard in range(n_rep * n_z):
            for a in range(2):
                arrived(act_slot(a, shard, part), act_recv.at[a, shard, part])

    last = (((1,), (1,)), ((), ()))
    first = (((0,), (0,)), ((), ()))

    def by_place(work):
        if not more:
            work(False)
        else:
            pl.when(inner)(lambda: work(True))
            pl.when(jnp.logical_not(inner))(lambda: work(False))

    def weights(full, kind, cols):
        rows = slice(2, 3) if kind else slice(0, 2)
        value = wa[rows, :, cols]
        value = value.reshape(-1, value.shape[-1])
        if full:
            extra = wa_more[rows, :, cols]
            value = jnp.concatenate([value, extra.reshape(-1, value.shape[-1])], axis=0)
        return value

    def contract(block, fresh):
        cols = span(block, depth)

        def work(full):
            for kind, ref, act in ((0, pre, xa), (1, pre_down, ca)):
                lhs = weights(full, kind, cols)
                part = lax.dot_general(lhs, act[:, cols], last, preferred_element_type=f32)
                rows = slice(0, lhs.shape[0])
                ref[rows] = part if fresh else ref[rows] + part

        by_place(work)

    for k in range(n_z):
        contract(at_z(near[k]), k == 0)
        for row in peers(y, n_y):
            for part in parts:
                w_arrived(part, at_z(near[k], row))
            contract(at_z(near[k], row), False)
    out.finish()

    def activate(side):
        cols = span(side, n_z * tokens)

        def rows_of(start, size, down):
            @pl.loop(0, size // 16)
            def _(step):
                gate = pl.ds(pl.multiple_of(start + step * 16, 16), 16)
                up = pl.ds(pl.multiple_of(start + size + step * 16, 16), 16)
                rows = pl.ds(pl.multiple_of(down + step * 16, 16), 16)
                gate_pre, up_pre, grad_hidden = pre[gate, cols], pre[up, cols], pre_down[rows, cols]
                sigmoid_gate = jax.nn.sigmoid(gate_pre)
                activated = gate_pre * sigmoid_gate
                ht[rows, cols] = (activated * up_pre).astype(bf16)
                gt[gate, cols] = (
                    grad_hidden * up_pre * sigmoid_gate * (1.0 + gate_pre * (1.0 - sigmoid_gate))
                ).astype(bf16)
                gt[up, cols] = (grad_hidden * activated).astype(bf16)

        rows_of(0, base, 0)
        if more:
            pl.when(inner)(lambda: rows_of(2 * base, more, base))

    def partial_inputs(side):
        rows = span(side, n_z * tokens)

        def work(full):
            rhs = weights(full, 0, slice(None))
            p[rows] = lax.dot_general(
                gt[: rhs.shape[0], rows], rhs, first, preferred_element_type=f32
            ).astype(bf16)

        by_place(work)
        for other in far_first:
            shard = side * n_z + other
            for j in range(1, n_tp):
                peer = lax.rem(tp + j, n_tp)
                out.send(
                    p.at[span(shard, tokens), span(peer, width)],
                    p_in.at[j - 1, shard],
                    p_recv.at[j - 1, shard],
                    "tp",
                    peer,
                )

    def pair_wait(shard):
        for j in range(n_tp - 1):
            arrived(p_in.at[j, shard], p_recv.at[j, shard])

    def pair_sum(shard):
        value = p[span(shard, tokens), span(tp, width)].astype(f32)
        for j in range(n_tp - 1):
            value = value + p_in[j, shard].astype(f32)
        return value

    def weight_block(block, dst, dst_more):
        cols = span(block, depth)

        def work(full):
            held = units if full else base
            both = jnp.dot(gt[: 2 * held], xa[:, cols], preferred_element_type=f32)
            down = jnp.dot(ht[:held], ca[:, cols], preferred_element_type=f32)
            dst[: 2 * base] = both[: 2 * base].astype(dst.dtype)
            dst[2 * base :] = down[:base].astype(dst.dtype)
            if full:
                dst_more[: 2 * more] = both[2 * base :].astype(dst.dtype)
                dst_more[2 * more :] = down[base:].astype(dst.dtype)

        by_place(work)

    def rep_sum(other):
        value = pair_sum(rep * n_z + other)
        for j in range(n_rep - 1):
            value = value + x_in[j, other].astype(f32)
        return value

    def rep_wait(other):
        for j in range(n_rep - 1):
            arrived(x_in.at[j, other], x_recv.at[j, other])

    def toward(other, passing):
        up = other > z
        came = jnp.where(up, 0, 1)
        behind = jnp.where(up, z >= 1, z + 1 < n_z)
        when = behind if passing else jnp.logical_not(behind)
        slot, recv_sem = z_in.at[came, other], z_recv.at[came, other]

        @pl.when(when)
        def _():
            rep_wait(other)
            value = rep_sum(other)
            if passing:
                arrived(slot, recv_sem)
                value = value + slot[...].astype(f32)
            r[other] = value.astype(bf16)

        peer = jnp.where(up, fs + n_y, fs - n_y)
        out.send(r.at[other], slot, recv_sem, "fs", peer, when)

    sets = [(gp, go, g_in, gs, dw)]
    if more:
        sets.append((gp_more, go_more, g_in_more, gs_more, dw_more))

    def dw_slot(extra, side, other):
        if extra:
            other = jnp.clip(other - 1, 0, n_z - 3)
            return dw_more.at[side * (n_z - 2) + other]
        return dw.at[side * n_z + other]

    def dw_send(extra, other, when):
        slot = dw_slot(extra, rep, other)
        for peer in peers(rep, n_rep):
            out.send(slot, slot, d_recv.at[extra, rep, other], "rep", peer, when)

    def g_step(other, own):
        def work(extra):
            partial, total, came, summed, _ = sets[extra]
            total = total[other]
            for j in range(n_y - 1):
                arrived(came.at[j, other], g_recv.at[extra, j, other])
                total = total + came[j, other].astype(f32)
            if own:
                dw_slot(extra, rep, z)[...] = total.astype(bf16)
            else:
                summed[other] = total.astype(bf16)

        for extra in range(len(sets)):
            if extra:
                pl.when(inner)(lambda: work(1))
            else:
                work(0)
            if own:
                dw_send(extra, z, here_too[extra])
            else:
                out.send(
                    sets[extra][3].at[other], dw_slot(extra, rep, z), d_recv.at[extra, rep, z],
                    "fs", at_z(other), here_too[extra],
                )

    def g_forward(other):
        for extra in range(len(sets)):
            when = inside(other) if extra else None
            arrived(dw_slot(extra, rep, other), d_recv.at[extra, rep, other], when)
            dw_send(extra, other, when)

    def to_row(other):
        for j in range(1, n_y):
            row = lax.rem(y + j, n_y)
            at = (j - 1, other)
            weight_block(at_z(other, row), gp.at[at], gp_more.at[at])
            for extra, (partial, _, came, *_) in enumerate(sets):
                out.send(
                    partial.at[at], came.at[at], g_recv.at[extra, j - 1, other],
                    "fs", at_z(z, row), here_too[extra],
                )

    def to_side(other):
        for j in range(1, n_rep):
            side = lax.rem(rep + j, n_rep)
            pair_wait(side * n_z + other)
            q[j - 1, other] = pair_sum(side * n_z + other).astype(bf16)
            out.send(
                q.at[j - 1, other], x_in.at[j - 1, other], x_recv.at[j - 1, other], "rep", side
            )

    for j in range(1, n_rep):
        side = lax.rem(rep + j, n_rep)
        activate(side)
        partial_inputs(side)
    activate(rep)
    rows = others[:-1] + [z] + others[-1:]
    to_row(rows[0])
    for other in far_first:
        to_side(other)
    for other in rows[1:]:
        to_row(other)
    partial_inputs(rep)
    for other in rows:
        weight_block(at_z(other), go.at[other], go_more.at[other])
    for other in far_first:
        pair_wait(rep * n_z + other)

    for other in others[:1]:
        toward(other, False)
    for other in others[:-1]:
        g_step(other, False)
    for other in others[:1]:
        toward(other, True)
    g_step(z, True)
    for other in others[1:2]:
        g_forward(other)
        toward(other, False)
    for other in others[-1:]:
        g_step(other, False)
    for other in others[2:]:
        toward(other, False)
    for other in others[:1]:
        g_forward(other)
    for other in others[1:][-1:]:
        toward(other, True)
    for other in others[2:]:
        g_forward(other)
    for other in others[1:-1]:
        toward(other, True)
    rep_wait(z)
    total[...] = rep_sum(z)
    for came, here in ((0, z >= 1), (1, z + 1 < n_z)):

        @pl.when(here)
        def _(came=came):
            arrived(z_in.at[came, z], z_recv.at[came, z])
            total[...] = total[...] + z_in[came, z].astype(f32)

    dx_ref[...] = total[...].astype(bf16)
    for side in peers(rep, n_rep):
        for other in [z] + others:
            for extra in range(len(sets)):
                arrived(
                    dw_slot(extra, side, other), d_recv.at[extra, side, other],
                    inside(other) if extra else None,
                )

    def gathered_rows(kind):
        rows = []
        for side in range(n_rep):
            for other in range(n_z):
                rows.append(dw[side * n_z + other, kind * base : (kind + 1) * base])
                if more and 0 < other < n_z - 1:
                    at = side * (n_z - 2) + other - 1
                    rows.append(dw_more[at, kind * more : (kind + 1) * more])
        return jnp.concatenate(rows, axis=0)

    dgate_ref[...] = gathered_rows(0).T
    dup_ref[...] = gathered_rows(1).T
    ddown_ref[...] = gathered_rows(2)
    out.finish()


VMEM = pl.BlockSpec(memory_space=pltpu.VMEM)
ANY = pl.BlockSpec(memory_space=pl.ANY)
DMA = pltpu.SemaphoreType.DMA


def fused(sizes, x, c, gate_weight, up_weight, down_weight):
    bf16, f32 = jnp.bfloat16, jnp.float32
    n_rep, n_fs, n_tp, n_y = sizes
    n_z = n_fs // n_y
    tokens, width = x.shape
    depth, hidden_tp = gate_weight.shape
    model, per_rep = width * n_tp, hidden_tp // n_rep
    base, more = per_rep // n_z, 0
    for size in range(16, per_rep, 16) if n_z > 2 else ():
        rest = per_rep - (n_z - 2) * size
        if rest % (16 * n_z) == 0 and 4 * size * n_z <= 3 * rest:
            base, more = rest // n_z, size
    units, spare, mids = base + more, max(more, 16), max(n_z - 2, 1)
    kinds = 4 if more else 2
    shards = n_rep * n_z
    group = shards * tokens
    tp_rep = n_tp + n_rep - 2
    n_sends = (
        2 * (2 + tp_rep) + 4 * ((n_z - 1) * (1 + tp_rep) - 1) + 2 * n_z * (n_rep - 1) * (n_tp - 1)
        + kinds * (n_y - 1) * n_z + 2 * kinds * (n_z - 1 + (n_z > 3))
    )
    grad_inputs, *grads = pl.pallas_call(
        functools.partial(layer_kernel, sizes),
        out_shape=(
            jax.ShapeDtypeStruct((tokens, width), bf16),
            jax.ShapeDtypeStruct((depth, hidden_tp), bf16),
            jax.ShapeDtypeStruct((depth, hidden_tp), bf16),
            jax.ShapeDtypeStruct((hidden_tp, depth), bf16),
        ),
        in_specs=[ANY] * 5,
        out_specs=(VMEM,) * 4,
        scratch_shapes=[
            *(pltpu.VMEM(v.shape, bf16) for v in (x, c, gate_weight, up_weight, down_weight)),
            DMA((5,)),
            pltpu.VMEM((group, model), bf16),
            pltpu.VMEM((group, model), bf16),
            pltpu.VMEM((2, hidden_tp, depth), bf16),
            pltpu.VMEM((3, base, model), bf16),
            pltpu.VMEM((3, spare, model), bf16),
            pltpu.VMEM((2 * units, group), f32),
            pltpu.VMEM((units, group), f32),
            pltpu.VMEM((2 * units, group), bf16),
            pltpu.VMEM((units, group), bf16),
            pltpu.VMEM((group, model), bf16),
            pltpu.VMEM((n_tp - 1, shards, tokens, width), bf16),
            pltpu.VMEM((n_rep - 1, n_z, tokens, width), bf16),
            pltpu.VMEM((n_rep - 1, n_z, tokens, width), bf16),
            pltpu.VMEM((n_z, tokens, width), bf16),
            pltpu.VMEM((2, n_z, tokens, width), bf16),
            pltpu.VMEM((tokens, width), f32),
            *(
                pltpu.VMEM((*lead, 3 * size, depth), kind)
                for size, places in ((base, shards), (spare, n_rep * mids))
                for lead, kind in (
                    ((n_y - 1, n_z), bf16), ((n_z,), f32), ((n_y - 1, n_z), bf16),
                    ((n_z,), bf16), ((places,), bf16),
                )
            ),
            DMA((n_sends,)),
            DMA((2, shards, n_tp)),
            DMA((kinds, n_fs)),
            DMA((n_tp - 1, shards)),
            DMA((n_rep - 1, n_z)),
            DMA((2, n_z)),
            DMA((kinds // 2, n_y - 1, n_z)),
            DMA((kinds // 2, n_rep, n_z)),
        ],
        compiler_params=pltpu.CompilerParams(
            collective_id=0, has_side_effects=True, vmem_limit_bytes=60 * 2**20
        ),
    )(x, c, gate_weight, up_weight, down_weight)
    return grad_inputs, *(v.astype(f32) for v in grads)


def gathered(x, c, gate_weight, up_weight, down_weight):
    bf16, f32 = jnp.bfloat16, jnp.float32
    last = (((1,), (1,)), ((), ()))
    first = (((0,), (0,)), ((), ()))
    x, c = (lax.all_gather(v, "tp", axis=1, tiled=True) for v in (x, c))
    gate, up = (lax.all_gather(v, "fs", axis=0, tiled=True) for v in (gate_weight, up_weight))
    down = lax.all_gather(down_weight, "fs", axis=1, tiled=True)
    gate_pre = jnp.dot(x, gate, preferred_element_type=f32)
    up_pre = jnp.dot(x, up, preferred_element_type=f32)
    grad_hidden = lax.dot_general(c, down, last, preferred_element_type=f32)
    sigmoid_gate = jax.nn.sigmoid(gate_pre)
    activated = gate_pre * sigmoid_gate
    hidden = (activated * up_pre).astype(bf16)
    grad_gate = (
        grad_hidden * up_pre * sigmoid_gate * (1.0 + gate_pre * (1.0 - sigmoid_gate))
    ).astype(bf16)
    grad_up = (grad_hidden * activated).astype(bf16)
    partial_sum = lax.dot_general(grad_gate, gate, last, preferred_element_type=f32)
    partial_sum += lax.dot_general(grad_up, up, last, preferred_element_type=f32)
    grad_inputs = lax.psum_scatter(partial_sum, "tp", scatter_dimension=1, tiled=True)

    def scattered(lhs, rhs, dimension):
        grads = lax.dot_general(lhs, rhs, first, preferred_element_type=f32)
        grads = lax.psum_scatter(grads, "fs", scatter_dimension=dimension, tiled=True)
        return lax.psum(grads, "rep")

    return (
        grad_inputs.astype(bf16),
        scattered(x, grad_gate, 0),
        scattered(x, grad_up, 0),
        scattered(hidden, c, 1),
    )


def per_device(n_rep, n_fs, n_tp, x, c, gate_weight, up_weight, down_weight):
    n_y = max(k for k in range(1, n_fs + 1) if n_fs % k == 0 and k * k <= n_fs)
    n_z = n_fs // n_y
    tokens, width = x.shape
    depth, hidden_tp = gate_weight.shape
    args = (x, c, gate_weight, up_weight, down_weight)
    whole = hidden_tp % (16 * n_rep * n_z) == 0
    if whole and tokens % 128 == width % 128 == depth % 128 == 0 and min(n_rep, n_y, n_tp) > 1:
        return fused((n_rep, n_fs, n_tp, n_y), *args)
    return gathered(*args)


def solution(mesh):
    n_rep, n_fs, n_tp = (mesh.shape[axis] for axis in ("rep", "fs", "tp"))
    placed = (
        P(("rep", "fs"), "tp"),
        P(("rep", "fs"), "tp"),
        P("fs", "tp"),
        P("fs", "tp"),
        P("tp", "fs"),
    )
    return jax.shard_map(
        functools.partial(per_device, n_rep, n_fs, n_tp),
        mesh=mesh,
        in_specs=placed,
        out_specs=(P(("rep", "fs"), "tp"), P("fs", "tp"), P("fs", "tp"), P("tp", "fs")),
        check_vma=False,
    )
```

time: 140 us -> 122 us (0.87)
  the two profiles are of different devices: /device:TPU:16 before, /device:TPU:0 now
where the time goes in v3:
time: 122 us
  Pallas kernels  115 us (94%)
  other arithmetic  4.77 us (4%)
    pallas_call x1, Pallas kernels, fused(): pl.pallas_call(functools.partial(layer_kernel, sizes), out_shape=(jax.Sha...  115 us
    convert_element_type x3, other arithmetic, fused(): return (grad_inputs, *(v.astype(f32) for v in grads))  4.77 us

profile of v3, /device:TPU:0, one launch (start us, length us, event | category | flops | bytes accessed | tf_op | source)
XLA Modules:
  0.0 121.6 jit_solution(12875051325237057246)
XLA Ops:
  0.6 115.3 %shard_map.84 = (bf16[128,1024]{1,0:T(8,128)(2,1)}, bf16[256,1408]{1,0:T(8,128)(2,1)}, bf16[256,1408]{1,0:T(8,128)(2,1)}, bf16[1408,256]{1,0:T(8,128)(2,1)}) custom-call(bf16[128,1024]{1,0:T(8,128)(2,1)} %refs_0_.1, bf16[128,1024]{1,0:T(8,128)(2,1)} %refs_1_.1, bf16[256,1408]{1,0:T(8,128)(2,1)} %refs_2_.1, bf16[256,1408]{1,0:T(8,128)(2,1)} %refs_3_.1, ...), custom_call_target="tpu_custom_call" | custom-call | tf_op jit(solution)/shard_map/pallas_call | solution.py:558
  116.0 0.0 copy-start.1
  116.0 2.4 %convert_element_type.9 = f32[256,1408]{1,0:T(8,128)} convert(bf16[256,1408]{1,0:T(8,128)(2,1)} %get-tuple-element.9) | non-fusion elementwise | flops 360448 | bytes 2162688 | tf_op jit(solution)/shard_map/convert_element_type | solution.py:608
  118.4 0.0 copy-done.1
  118.4 0.0 copy-start
  118.4 1.2 convert_element_type.10
  119.6 0.2 copy-done
  119.7 0.0 copy-start.2
  119.7 1.2 convert_element_type.11
  120.9 0.0 copy-done.2
  120.9 0.7 copy.10
Async XLA Ops:
  116.0 2.4 %copy-start.1 = (bf16[256,1408]{1,0:T(8,128)(2,1)S(1)}, bf16[256,1408]{1,0:T(8,128)(2,1)}, u32[]{:S(2)}) copy-start(bf16[256,1408]{1,0:T(8,128)(2,1)} %get-tuple-element.10) | copy-start | bytes 2162692
  118.4 1.4 %copy-start = (bf16[1408,256]{1,0:T(8,128)(2,1)S(1)}, bf16[1408,256]{1,0:T(8,128)(2,1)}, u32[]{:S(2)}) copy-start(bf16[1408,256]{1,0:T(8,128)(2,1)} %get-tuple-element.11) | copy-start | bytes 2162692
  119.7 1.2 copy-start.2

commit v4 on v3

--- a/solution.py
+++ b/solution.py
@@ -124,6 +124,11 @@
         low, high = jnp.where(above, low, low + 1), jnp.where(above, high - 1, high)
     others = far_first[:-1]
     near = [z] + others[::-1]
+    halves = 1 if n_z % 2 else 2
+    half = n_z // halves
+    start = z // half * half
+    home = [start + lax.rem(z - start + i, half) for i in range(half)]
+    away = [jnp.where(z < half, n_z - 1 - i, i) for i in range(n_z - half)]
 
     own_acts, acts = (x_ref, c_ref), (xa, ca)
 
@@ -232,6 +237,8 @@
                 to_tp(a, shard, slot, here)
             if k == n_z - 1 and a == 0:
                 send_weights(k)
+                for other in home[1:]:
+                    from_rep(other)
         if k < n_z - 2 or not held and k == n_z - 2:
             send_weights(k)
         if k == 1:
@@ -242,16 +249,18 @@
     if n_z == 1:
         from_rep(z)
     if held:
+        near[2], near[3] = near[3], near[2]
         swap_weights(near[2])
+        swap_weights(near[3])
         send_weights(n_z - 2, inside(z))
-    for k in range(3 if held else 1, n_z):
+    for k in range(4 if held else 1, n_z):
         swap_weights(near[k])
-    for k in range(1, n_z):
-        from_rep(near[k])
-    for part in peers(tp, n_tp):
-        for shard in range(n_rep * n_z):
-            for a in range(2):
-                arrived(act_slot(a, shard, part), act_recv.at[a, shard, part])
+    def acts_arrived(side, places):
+        for part in peers(tp, n_tp):
+            for other in places:
+                for a in range(2):
+                    shard = side * n_z + other
+                    arrived(act_slot(a, shard, part), act_recv.at[a, shard, part])
 
     last = (((1,), (1,)), ((), ()))
     first = (((0,), (0,)), ((), ()))
@@ -272,28 +281,49 @@
             value = jnp.concatenate([value, extra.reshape(-1, value.shape[-1])], axis=0)
         return value
 
-    def contract(block, fresh):
+    def tokens_of(side, away):
+        place = z // half
+        return span(side * halves + (1 - place if away else place), half * tokens)
+
+    def contract(block, groups, fresh):
         cols = span(block, depth)
 
         def work(full):
             for kind, ref, act in ((0, pre, xa), (1, pre_down, ca)):
                 lhs = weights(full, kind, cols)
-                part = lax.dot_general(lhs, act[:, cols], last, preferred_element_type=f32)
                 rows = slice(0, lhs.shape[0])
-                ref[rows] = part if fresh else ref[rows] + part
+                for group in groups:
+                    at = tokens_of(*group)
+                    part = lax.dot_general(lhs, act[at, cols], last, preferred_element_type=f32)
+                    ref[rows, at] = part if fresh else ref[rows, at] + part
 
         by_place(work)
 
+    sides = peers(rep, n_rep)
+    soon = [(side, False) for side in sides + [rep]]
+    late = []
+    for side in sides + [rep]:
+        acts_arrived(side, home)
+    if away:
+        acts_arrived(rep, away)
+        soon.append((rep, True))
+        late = [(side, True) for side in sides]
+    blocks = []
     for k in range(n_z):
-        contract(at_z(near[k]), k == 0)
+        if k == n_z // 2:
+            for other in away:
+                from_rep(other)
+        blocks.append(at_z(near[k]))
+        contract(blocks[-1], soon, k == 0)
         for row in peers(y, n_y):
+            blocks.append(at_z(near[k], row))
             for part in parts:
-                w_arrived(part, at_z(near[k], row))
-            contract(at_z(near[k], row), False)
+                w_arrived(part, blocks[-1])
+            contract(blocks[-1], soon, False)
     out.finish()
 
-    def activate(side):
-        cols = span(side, n_z * tokens)
+    def activate(group):
+        cols = tokens_of(*group)
 
         def rows_of(start, size, down):
             @pl.loop(0, size // 16)
@@ -314,8 +344,8 @@
         if more:
             pl.when(inner)(lambda: rows_of(2 * base, more, base))
 
-    def partial_inputs(side):
-        rows = span(side, n_z * tokens)
+    def partial_inputs(group):
+        rows = tokens_of(*group)
 
         def work(full):
             rhs = weights(full, 0, slice(None))
@@ -324,8 +354,8 @@
             ).astype(bf16)
 
         by_place(work)
-        for other in far_first:
-            shard = side * n_z + other
+        for other in away if group[1] else home[1:] + home[:1]:
+            shard = group[0] * n_z + other
             for j in range(1, n_tp):
                 peer = lax.rem(tp + j, n_tp)
                 out.send(
@@ -456,27 +486,37 @@
                 q.at[j - 1, other], x_in.at[j - 1, other], x_recv.at[j - 1, other], "rep", side
             )
 
-    for j in range(1, n_rep):
-        side = lax.rem(rep + j, n_rep)
-        activate(side)
-        partial_inputs(side)
-    activate(rep)
+    for group in soon[: len(sides)]:
+        activate(group)
+        partial_inputs(group)
+    for group in soon[len(sides) :]:
+        activate(group)
+    for side, _ in late:
+        acts_arrived(side, away)
+    for i, block in enumerate(blocks if late else ()):
+        contract(block, late, i == 0)
+    for other in home[1:]:
+        to_side(other)
+    for group in late:
+        activate(group)
+        partial_inputs(group)
     rows = others[:-1] + [z] + others[-1:]
     to_row(rows[0])
-    for other in far_first:
+    for other in away + [z]:
         to_side(other)
     for other in rows[1:]:
         to_row(other)
-    partial_inputs(rep)
+    for group in soon[len(sides) :]:
+        partial_inputs(group)
     for other in rows:
         weight_block(at_z(other), go.at[other], go_more.at[other])
     for other in far_first:
         pair_wait(rep * n_z + other)
 
-    for other in others[:1]:
-        toward(other, False)
-    for other in others[:-1]:
+    for i, other in enumerate(others[:-1]):
         g_step(other, False)
+        if i == 0:
+            toward(other, False)
     for other in others[:1]:
         toward(other, True)
     g_step(z, True)
@@ -534,6 +574,11 @@
 DMA = pltpu.SemaphoreType.DMA
 
 
+def widen_kernel(*refs):
+    for src, dst in zip(refs[:4], refs[4:]):
+        dst[...] = src[...].astype(dst.dtype)
+
+
 def fused(sizes, x, c, gate_weight, up_weight, down_weight):
     bf16, f32 = jnp.bfloat16, jnp.float32
     n_rep, n_fs, n_tp, n_y = sizes
@@ -544,7 +589,7 @@
     base, more = per_rep // n_z, 0
     for size in range(16, per_rep, 16) if n_z > 2 else ():
         rest = per_rep - (n_z - 2) * size
-        if rest % (16 * n_z) == 0 and 4 * size * n_z <= 3 * rest:
+        if rest % (16 * n_z) == 0 and 4 * size * n_z <= 5 * rest:
             base, more = rest // n_z, size
     units, spare, mids = base + more, max(more, 16), max(n_z - 2, 1)
     kinds = 4 if more else 2
@@ -605,7 +650,21 @@
             collective_id=0, has_side_effects=True, vmem_limit_bytes=60 * 2**20
         ),
     )(x, c, gate_weight, up_weight, down_weight)
-    return grad_inputs, *(v.astype(f32) for v in grads)
+    steps = 2
+
+    def block(shape):
+        return pl.BlockSpec((shape[0] // steps, shape[1]), lambda i: (i, 0))
+
+    results = (grad_inputs, *grads)
+    return pl.pallas_call(
+        widen_kernel,
+        grid=(steps,),
+        out_shape=[
+            jax.ShapeDtypeStruct(v.shape, f32 if i else bf16) for i, v in enumerate(results)
+        ],
+        in_specs=[block(v.shape) for v in results],
+        out_specs=[block(v.shape) for v in results],
+    )(*results)
 
 
 def gathered(x, c, gate_weight, up_weight, down_weight):

time: 122 us -> 116 us (0.951)
  other arithmetic: 4.77 us -> 0 us
    convert_element_type x3 -> x0, other arithmetic: 4.77 us -> none  [fused(): return (grad_inputs, *(v.astype(f32) for v in grads))]
    pallas_call x0 -> x1, Pallas kernels: none -> 3.51 us  [fused(): pl.pallas_call(widen_kernel, grid=(steps,), out_shape=[jax.ShapeDtypeStru...]
    pallas_call x1, Pallas kernels: 115 us -> 112 us  [fused(): pl.pallas_call(functools.partial(layer_kernel, sizes), out_shape=(jax.Sha...]
where the time goes in v4:
time: 116 us
  Pallas kernels  115 us (99%)
    pallas_call x1, Pallas kernels, fused(): pl.pallas_call(functools.partial(layer_kernel, sizes), out_shape=(jax.Sha...  112 us
    pallas_call x1, Pallas kernels, fused(): pl.pallas_call(widen_kernel, grid=(steps,), out_shape=[jax.ShapeDtypeStru...  3.51 us

profile of v4, /device:TPU:0, one launch (start us, length us, event | category | flops | bytes accessed | tf_op | source)
XLA Modules:
  0.0 116.0 jit_solution(14239640843388951072)
XLA Ops:
  0.6 111.9 %shard_map.84 = (bf16[128,1024]{1,0:T(8,128)(2,1)}, bf16[256,1408]{1,0:T(8,128)(2,1)}, bf16[256,1408]{1,0:T(8,128)(2,1)}, bf16[1408,256]{1,0:T(8,128)(2,1)}) custom-call(bf16[128,1024]{1,0:T(8,128)(2,1)} %refs_0_.1, bf16[128,1024]{1,0:T(8,128)(2,1)} %refs_1_.1, bf16[256,1408]{1,0:T(8,128)(2,1)} %refs_2_.1, bf16[256,1408]{1,0:T(8,128)(2,1)} %refs_3_.1, ...), custom_call_target="tpu_custom_call" | custom-call | tf_op jit(solution)/shard_map/pallas_call | solution.py:603
  112.5 3.5 %shard_map.85 = (bf16[128,1024]{1,0:T(8,128)(2,1)}, f32[256,1408]{1,0:T(8,128)}, f32[256,1408]{1,0:T(8,128)}, f32[1408,256]{1,0:T(8,128)}) custom-call(bf16[128,1024]{1,0:T(8,128)(2,1)} %get-tuple-element.8.refs_0_, bf16[256,1408]{1,0:T(8,128)(2,1)} %get-tuple-element.9.refs_1_, bf16[256,1408]{1,0:T(8,128)(2,1)} %get-tuple-element.10.refs_2_, ...), custom_call_target="tpu_custom_call" | custom-call | tf_op jit(solution)/shard_map/pallas_call | solution.py:659

commit v5 on v4

--- a/solution.py
+++ b/solution.py
@@ -93,9 +93,9 @@
 def layer(
     sizes, copies, x_ref, c_ref, gate_ref, up_ref, down_ref, dx_ref, dgate_ref, dup_ref, ddown_ref,
     xa, ca, wt, wa, wa_more, pre, pre_down, gt, ht,
-    p, p_in, q, x_in, r, z_in, total,
+    p, p_in, q, x_in, r, z_in, total, h, h_in,
     gp, go, g_in, gs, dw, gp_more, go_more, g_in_more, gs_more, dw_more,
-    sends, act_recv, w_recv, p_recv, x_recv, z_recv, g_recv, d_recv,
+    sends, act_recv, w_recv, p_recv, x_recv, z_recv, g_recv, d_recv, h_recv,
 ):
     n_rep, n_fs, n_tp, n_y = sizes
     n_z = n_fs // n_y
@@ -146,13 +146,13 @@
         for peer in peers(tp, n_tp):
             act_send(a, shard, src, "tp", peer, when)
 
-    def from_rep(other):
+    def from_rep(other, only=None):
         for peer in peers(rep, n_rep):
             for a in range(2):
                 shard = peer * n_z + other
                 slot = act_slot(a, shard, tp)
-                arrived(slot, act_recv.at[a, shard, tp])
-                to_tp(a, shard, slot)
+                arrived(slot, act_recv.at[a, shard, tp], only)
+                to_tp(a, shard, slot, only)
 
     mine = rep * n_z + z
     for a in range(2):
@@ -238,7 +238,7 @@
             if k == n_z - 1 and a == 0:
                 send_weights(k)
                 for other in home[1:]:
-                    from_rep(other)
+                    from_rep(other, jnp.logical_not(inside(z)) if held else None)
         if k < n_z - 2 or not held and k == n_z - 2:
             send_weights(k)
         if k == 1:
@@ -251,6 +251,8 @@
     if held:
         near[2], near[3] = near[3], near[2]
         swap_weights(near[2])
+        for other in home[1:]:
+            from_rep(other, inside(z))
         swap_weights(near[3])
         send_weights(n_z - 2, inside(z))
     for k in range(4 if held else 1, n_z):
@@ -391,9 +393,14 @@
 
         by_place(work)
 
-    def rep_sum(other):
+    paired = n_z == 4
+    if paired:
+        taken = jnp.where(inside(z), away[0], away[1])
+        given = jnp.where(inside(z), away[1], away[0])
+
+    def rep_sum(other, from_sides=True):
         value = pair_sum(rep * n_z + other)
-        for j in range(n_rep - 1):
+        for j in range(n_rep - 1 if from_sides else 0):
             value = value + x_in[j, other].astype(f32)
         return value
 
@@ -401,7 +408,9 @@
         for j in range(n_rep - 1):
             arrived(x_in.at[j, other], x_recv.at[j, other])
 
-    def toward(other, passing):
+    def toward(i, passing):
+        other = others[i]
+        from_sides = not paired or i == 2 or passing == (i == 0)
         up = other > z
         came = jnp.where(up, 0, 1)
         behind = jnp.where(up, z >= 1, z + 1 < n_z)
@@ -410,8 +419,9 @@
 
         @pl.when(when)
         def _():
-            rep_wait(other)
-            value = rep_sum(other)
+            if from_sides:
+                rep_wait(other)
+            value = rep_sum(other, from_sides)
             if passing:
                 arrived(slot, recv_sem)
                 value = value + slot[...].astype(f32)
@@ -477,14 +487,35 @@
                     "fs", at_z(z, row), here_too[extra],
                 )
 
-    def to_side(other):
+    def to_side(other, only=None):
         for j in range(1, n_rep):
             side = lax.rem(rep + j, n_rep)
-            pair_wait(side * n_z + other)
-            q[j - 1, other] = pair_sum(side * n_z + other).astype(bf16)
+
+            def work(j=j, side=side):
+                if only is None:
+                    pair_wait(side * n_z + other)
+                value = pair_sum(side * n_z + other)
+                if only is not None:
+                    arrived(h_in.at[j - 1], h_recv.at[j - 1])
+                    value = value + h_in[j - 1].astype(f32)
+                q[j - 1, other] = value.astype(bf16)
+
+            if only is None:
+                work()
+            else:
+                pl.when(only)(work)
             out.send(
-                q.at[j - 1, other], x_in.at[j - 1, other], x_recv.at[j - 1, other], "rep", side
+                q.at[j - 1, other], x_in.at[j - 1, other], x_recv.at[j - 1, other],
+                "rep", side, only,
             )
+
+    def give():
+        for j in range(1, n_rep):
+            side = lax.rem(rep + j, n_rep)
+            for other in away:
+                pair_wait(side * n_z + other)
+            h[j - 1] = pair_sum(side * n_z + given).astype(bf16)
+            out.send(h.at[j - 1], h_in.at[j - 1], h_recv.at[j - 1], "fs", at_z(home[1]))
 
     for group in soon[: len(sides)]:
         activate(group)
@@ -502,7 +533,10 @@
         partial_inputs(group)
     rows = others[:-1] + [z] + others[-1:]
     to_row(rows[0])
-    for other in away + [z]:
+    if paired:
+        to_side(z)
+        give()
+    for other in [] if paired else away + [z]:
         to_side(other)
     for other in rows[1:]:
         to_row(other)
@@ -513,28 +547,35 @@
     for other in far_first:
         pair_wait(rep * n_z + other)
 
+    count = len(others)
+    if paired:
+        toward(0, False)
     for i, other in enumerate(others[:-1]):
         g_step(other, False)
-        if i == 0:
-            toward(other, False)
-    for other in others[:1]:
-        toward(other, True)
+        if paired:
+            to_side(taken, inside(z) if i == 0 else jnp.logical_not(inside(z)))
+        elif i == 0:
+            toward(0, False)
+    if count == 1:
+        toward(0, False)
+    if count:
+        toward(0, True)
     g_step(z, True)
-    for other in others[1:2]:
-        g_forward(other)
-        toward(other, False)
     for other in others[-1:]:
         g_step(other, False)
-    for other in others[2:]:
-        toward(other, False)
+    if count > 1:
+        g_forward(others[1])
+        toward(1, False)
+    for i in range(2, count):
+        toward(i, False)
     for other in others[:1]:
         g_forward(other)
-    for other in others[1:][-1:]:
-        toward(other, True)
+    if count > 1:
+        toward(count - 1, True)
     for other in others[2:]:
         g_forward(other)
-    for other in others[1:-1]:
-        toward(other, True)
+    for i in range(1, count - 1):
+        toward(i, True)
     rep_wait(z)
     total[...] = rep_sum(z)
     for came, here in ((0, z >= 1), (1, z + 1 < n_z)):
@@ -589,7 +630,7 @@
     base, more = per_rep // n_z, 0
     for size in range(16, per_rep, 16) if n_z > 2 else ():
         rest = per_rep - (n_z - 2) * size
-        if rest % (16 * n_z) == 0 and 4 * size * n_z <= 5 * rest:
+        if rest % (16 * n_z) == 0 and 4 * size * n_z <= 3 * rest:
             base, more = rest // n_z, size
     units, spare, mids = base + more, max(more, 16), max(n_z - 2, 1)
     kinds = 4 if more else 2
@@ -597,7 +638,7 @@
     group = shards * tokens
     tp_rep = n_tp + n_rep - 2
     n_sends = (
-        2 * (2 + tp_rep) + 4 * ((n_z - 1) * (1 + tp_rep) - 1) + 2 * n_z * (n_rep - 1) * (n_tp - 1)
+        2 * (2 + tp_rep) + 4 * ((n_z - 1) * (1 + tp_rep) - 1) + 2 * (n_z + n_z // 2) * (n_rep - 1) * (n_tp - 1)
         + kinds * (n_y - 1) * n_z + 2 * kinds * (n_z - 1 + (n_z > 3))
     )
     grad_inputs, *grads = pl.pallas_call(
@@ -629,6 +670,8 @@
             pltpu.VMEM((n_z, tokens, width), bf16),
             pltpu.VMEM((2, n_z, tokens, width), bf16),
             pltpu.VMEM((tokens, width), f32),
+            pltpu.VMEM((n_rep - 1, tokens, width), bf16),
+            pltpu.VMEM((n_rep - 1, tokens, width), bf16),
             *(
                 pltpu.VMEM((*lead, 3 * size, depth), kind)
                 for size, places in ((base, shards), (spare, n_rep * mids))
@@ -645,6 +688,7 @@
             DMA((2, n_z)),
             DMA((kinds // 2, n_y - 1, n_z)),
             DMA((kinds // 2, n_rep, n_z)),
+            DMA((n_rep - 1,)),
         ],
         compiler_params=pltpu.CompilerParams(
             collective_id=0, has_side_effects=True, vmem_limit_bytes=60 * 2**20

time: 116 us -> 113 us (0.974)
  Pallas kernels: 115 us -> 112 us
    pallas_call x1, Pallas kernels: 112 us -> 109 us  [fused(): pl.pallas_call(functools.partial(layer_kernel, sizes), out_shape=(jax.Sha...]
where the time goes in v5:
time: 113 us
  Pallas kernels  112 us (99%)
    pallas_call x1, Pallas kernels, fused(): pl.pallas_call(functools.partial(layer_kernel, sizes), out_shape=(jax.Sha...  109 us
    pallas_call x1, Pallas kernels, fused(): pl.pallas_call(widen_kernel, grid=(steps,), out_shape=[jax.ShapeDtypeStru...  3.51 us

profile of v5, /device:TPU:0, one launch (start us, length us, event | category | flops | bytes accessed | tf_op | source)
XLA Modules:
  0.0 112.7 jit_solution(2672222185185790016)
XLA Ops:
  0.6 108.6 %shard_map.84 = (bf16[128,1024]{1,0:T(8,128)(2,1)}, bf16[256,1408]{1,0:T(8,128)(2,1)}, bf16[256,1408]{1,0:T(8,128)(2,1)}, bf16[1408,256]{1,0:T(8,128)(2,1)}) custom-call(bf16[128,1024]{1,0:T(8,128)(2,1)} %refs_0_.1, bf16[128,1024]{1,0:T(8,128)(2,1)} %refs_1_.1, bf16[256,1408]{1,0:T(8,128)(2,1)} %refs_2_.1, bf16[256,1408]{1,0:T(8,128)(2,1)} %refs_3_.1, ...), custom_call_target="tpu_custom_call" | custom-call | tf_op jit(solution)/shard_map/pallas_call | solution.py:644
  109.2 3.5 %shard_map.85 = (bf16[128,1024]{1,0:T(8,128)(2,1)}, f32[256,1408]{1,0:T(8,128)}, f32[256,1408]{1,0:T(8,128)}, f32[1408,256]{1,0:T(8,128)}) custom-call(bf16[128,1024]{1,0:T(8,128)(2,1)} %get-tuple-element.8.refs_0_, bf16[256,1408]{1,0:T(8,128)(2,1)} %get-tuple-element.9.refs_1_, bf16[256,1408]{1,0:T(8,128)(2,1)} %get-tuple-element.10.refs_2_, ...), custom_call_target="tpu_custom_call" | custom-call | tf_op jit(solution)/shard_map/pallas_call | solution.py:703

commit v6 on v5

--- a/solution.py
+++ b/solution.py
@@ -526,13 +526,14 @@
         acts_arrived(side, away)
     for i, block in enumerate(blocks if late else ()):
         contract(block, late, i == 0)
+    for group in late:
+        activate(group)
+    rows = others[:-1] + [z] + others[-1:]
+    to_row(rows[0])
     for other in home[1:]:
         to_side(other)
     for group in late:
-        activate(group)
         partial_inputs(group)
-    rows = others[:-1] + [z] + others[-1:]
-    to_row(rows[0])
     if paired:
         to_side(z)
         give()

time: 113 us -> 112 us (level)
    pallas_call x1, Pallas kernels: 109 us -> 107 us  [fused(): pl.pallas_call(functools.partial(layer_kernel, sizes), out_shape=(jax.Sha...]
where the time goes in v6:
time: 112 us; the launch traced here: 111 us
  Pallas kernels  111 us (99%)
    pallas_call x1, Pallas kernels, fused(): pl.pallas_call(functools.partial(layer_kernel, sizes), out_shape=(jax.Sha...  107 us
    pallas_call x1, Pallas kernels, fused(): pl.pallas_call(widen_kernel, grid=(steps,), out_shape=[jax.ShapeDtypeStru...  3.51 us

profile of v6, /device:TPU:0, one launch (start us, length us, event | category | flops | bytes accessed | tf_op | source)
XLA Modules:
  0.0 111.5 jit_solution(11011993071962700239)
XLA Ops:
  0.6 107.3 %shard_map.84 = (bf16[128,1024]{1,0:T(8,128)(2,1)}, bf16[256,1408]{1,0:T(8,128)(2,1)}, bf16[256,1408]{1,0:T(8,128)(2,1)}, bf16[1408,256]{1,0:T(8,128)(2,1)}) custom-call(bf16[128,1024]{1,0:T(8,128)(2,1)} %refs_0_.1, bf16[128,1024]{1,0:T(8,128)(2,1)} %refs_1_.1, bf16[256,1408]{1,0:T(8,128)(2,1)} %refs_2_.1, bf16[256,1408]{1,0:T(8,128)(2,1)} %refs_3_.1, ...), custom_call_target="tpu_custom_call" | custom-call | tf_op jit(solution)/shard_map/pallas_call | solution.py:645
  108.0 3.5 %shard_map.85 = (bf16[128,1024]{1,0:T(8,128)(2,1)}, f32[256,1408]{1,0:T(8,128)}, f32[256,1408]{1,0:T(8,128)}, f32[1408,256]{1,0:T(8,128)}) custom-call(bf16[128,1024]{1,0:T(8,128)(2,1)} %get-tuple-element.8.refs_0_, bf16[256,1408]{1,0:T(8,128)(2,1)} %get-tuple-element.9.refs_1_, bf16[256,1408]{1,0:T(8,128)(2,1)} %get-tuple-element.10.refs_2_, ...), custom_call_target="tpu_custom_call" | custom-call | tf_op jit(solution)/shard_map/pallas_call | solution.py:704

commit v7 on v6

--- a/solution.py
+++ b/solution.py
@@ -210,7 +210,10 @@
         acts[a][span(mine, tokens), span(tp, width)] = own_acts[a][...]
 
     def send_weights(step, only=None):
-        for sign, here in ((1, z + step < n_z), (-1, z >= step)):
+        ways = [(1, z + step < n_z), (-1, z >= step)]
+        if 2 * step >= n_z:
+            ways = [(jnp.where(ways[0][1], 1, -1), jnp.logical_or(ways[0][1], ways[1][1]))]
+        for sign, here in ways:
             other = z + sign * step
             here = here if only is None else jnp.logical_and(here, only)
             for part in parts:
@@ -227,7 +230,12 @@
     held = n_z > 3
     for k in range(1, n_z):
         for a in range(2):
-            for here, onward, step in ((z >= k, z + 1 < n_z, -1), (z + k < n_z, z >= 1, 1)):
+            ways = [(z >= k, z + 1 < n_z, -1), (z + k < n_z, z >= 1, 1)]
+            if 2 * k >= n_z:
+                up = z >= k
+                here, onward = jnp.logical_or(up, z + k < n_z), jnp.where(up, z + 1, n_z - z) < n_z
+                ways = [(here, onward, jnp.where(up, -1, 1))]
+            for here, onward, step in ways:
                 shard = mine + step * k
                 slot = act_slot(a, shard, tp)
                 arrived(slot, act_recv.at[a, shard, tp], here)
@@ -638,9 +646,10 @@
     shards = n_rep * n_z
     group = shards * tokens
     tp_rep = n_tp + n_rep - 2
+    ways = sum(2 - (2 * k >= n_z) for k in range(1, n_z))
     n_sends = (
-        2 * (2 + tp_rep) + 4 * ((n_z - 1) * (1 + tp_rep) - 1) + 2 * (n_z + n_z // 2) * (n_rep - 1) * (n_tp - 1)
-        + kinds * (n_y - 1) * n_z + 2 * kinds * (n_z - 1 + (n_z > 3))
+        2 * (2 + tp_rep) + 2 * (ways * (1 + tp_rep) - 1) + 2 * (n_z + n_z // 2) * (n_rep - 1) * (n_tp - 1)
+        + kinds * (n_y - 1) * n_z + kinds * (ways + (n_z > 3))
     )
     grad_inputs, *grads = pl.pallas_call(
         functools.partial(layer_kernel, sizes),

time: 112 us -> 111 us (level)
  no operation moved by 1% of the time
where the time goes in v7:
time: 111 us
  Pallas kernels  111 us (100%)
    pallas_call x1, Pallas kernels, fused(): pl.pallas_call(functools.partial(layer_kernel, sizes), out_shape=(jax.Sha...  107 us
    pallas_call x1, Pallas kernels, fused(): pl.pallas_call(widen_kernel, grid=(steps,), out_shape=[jax.ShapeDtypeStru...  3.51 us

profile of v7, /device:TPU:0, one launch (start us, length us, event | category | flops | bytes accessed | tf_op | source)
XLA Modules:
  0.0 111.2 jit_solution(8608371773986519381)
XLA Ops:
  0.6 107.1 %shard_map.84 = (bf16[128,1024]{1,0:T(8,128)(2,1)}, bf16[256,1408]{1,0:T(8,128)(2,1)}, bf16[256,1408]{1,0:T(8,128)(2,1)}, bf16[1408,256]{1,0:T(8,128)(2,1)}) custom-call(bf16[128,1024]{1,0:T(8,128)(2,1)} %refs_0_.1, bf16[128,1024]{1,0:T(8,128)(2,1)} %refs_1_.1, bf16[256,1408]{1,0:T(8,128)(2,1)} %refs_2_.1, bf16[256,1408]{1,0:T(8,128)(2,1)} %refs_3_.1, ...), custom_call_target="tpu_custom_call" | custom-call | tf_op jit(solution)/shard_map/pallas_call | solution.py:654
  107.7 3.5 %shard_map.85 = (bf16[128,1024]{1,0:T(8,128)(2,1)}, f32[256,1408]{1,0:T(8,128)}, f32[256,1408]{1,0:T(8,128)}, f32[1408,256]{1,0:T(8,128)}) custom-call(bf16[128,1024]{1,0:T(8,128)(2,1)} %get-tuple-element.8.refs_0_, bf16[256,1408]{1,0:T(8,128)(2,1)} %get-tuple-element.9.refs_1_, bf16[256,1408]{1,0:T(8,128)(2,1)} %get-tuple-element.10.refs_2_, ...), custom_call_target="tpu_custom_call" | custom-call | tf_op jit(solution)/shard_map/pallas_call | solution.py:713
